TPU v7x, 512 devices: a whole 4x8x8 slice. The times are simulated.
512 devices in a mesh: fs: 128 (over z, y, core), tp: 4 (over x).
Axes of the slice: x: 4, y: 8, z: 8, core: 2. Of those that a mesh axis runs over, the one named last changes fastest.
Arguments:
- saved_input: bfloat16 [98304, 2048], P('fs'), may hold values from -24 to 24
- cot_inproj: bfloat16 [98304, 1024], P('fs', 'tp'), may hold values from -0.019042969 to 0.019042969
- cot_outproj: bfloat16 [98304, 1024], P('fs', 'tp'), may hold values from -0.019042969 to 0.019042969
- factor_inproj: bfloat16 [2048, 256], P('fs')
- factor_outproj: bfloat16 [2048, 256], P('fs')
- weight_inproj: float32 [2048, 1024], P('fs', 'tp'), may hold values from -0.125 to 0.125
- weight_outproj: float32 [2048, 1024], P('fs', 'tp'), may hold values from -0.125 to 0.125
- first_inproj: float32 [256, 1024], P('fs', 'tp'), may hold values from -6 to 6
- first_outproj: float32 [256, 1024], P('fs', 'tp'), may hold values from -6 to 6
- second_inproj: float32 [256, 1024], P('fs', 'tp'), may hold values from 0.25 to 4
- second_outproj: float32 [256, 1024], P('fs', 'tp'), may hold values from 0.25 to 4
Outputs:
- update_inproj: float32 [2048, 1024], P('fs', 'tp')
- update_outproj: float32 [2048, 1024], P('fs', 'tp')
- new_inproj: float32 [2048, 1024], P('fs', 'tp')
- new_outproj: float32 [2048, 1024], P('fs', 'tp')
- copy_inproj: bfloat16 [2048, 1024], P(None, 'tp')
- copy_outproj: bfloat16 [2048, 1024], P(None, 'tp')
- first_inproj_new: float32 [256, 1024], P('fs', 'tp')
- first_outproj_new: float32 [256, 1024], P('fs', 'tp')
- second_inproj_new: float32 [256, 1024], P('fs', 'tp')
- second_outproj_new: float32 [256, 1024], P('fs', 'tp')
All inputs are finite; a program needn't handle non-finite values.
Results may differ from a plain program's by a relative error of at most 0.00045.
Values may be sent and summed in bfloat16 or wider, within the bound.
A program may use at most 64 MiB of HBM per device.

v0:
```python
import jax
import jax.numpy as jnp
from jax import lax
from jax.sharding import Mesh
from jax.sharding import PartitionSpec as P

FS = ("fs_0", "fs_1", "fs_2")


def from_everyone(value, axis):
    length = lax.axis_size(axis)
    return lax.all_to_all(
        jnp.broadcast_to(value[None], (length, *value.shape)), axis, 0, 0, tiled=True
    )


def in_order(blocks, dim):
    dims = list(blocks.shape[1:])
    dims[dim] *= blocks.shape[0]
    return jnp.moveaxis(blocks, 0, dim).reshape(dims)


def gathered_by_axis(value, axes, dim):
    far, near = axes
    initial = from_everyone(value, far)
    blocks = jnp.swapaxes(from_everyone(initial, near), 0, 1)
    return in_order(blocks.reshape(-1, *value.shape), dim)


def side_by_side(arrays, axis, dim, along):
    ends, at = ([], 0)
    for a in arrays[:-1]:
        at += a.shape[along]
        ends.append(at)
    both = jnp.concatenate(arrays, axis=along)
    return tuple(jnp.split(gathered_by_axis(both, axis, dim), ends, axis=along))


def in_blocks(value, dim, length):
    before, after = (value.shape[:dim], value.shape[dim + 1 :])
    return jnp.moveaxis(value.reshape(*before, length, -1, *after), dim, 0)


def summed_on_arrival(value, axis, dim):
    blocks = in_blocks(value, dim, lax.axis_size(axis))
    arrived = lax.all_to_all(blocks, axis, split_axis=0, concat_axis=0, tiled=True)
    return arrived.sum(axis=0)


def sum_by_axis(value, axes, dim):
    far, near = axes
    own = summed_on_arrival(in_blocks(value, dim, lax.axis_size(far)), near, dim + 1)
    return jnp.sum(lax.all_to_all(own, far, 0, 0, tiled=True), axis=0)


def sent_together(arrays, axis, dim, along):
    both = jnp.concatenate(arrays, axis=along)
    filled, at, outs = (sum_by_axis(both, axis, dim), 0, [])
    for a in arrays:
        outs.append(lax.slice_in_dim(filled, at, at + a.shape[along], axis=along))
        at += a.shape[along]
    return tuple(outs)


def taken_together(value, axis):
    return from_everyone(value, axis).sum(axis=0)


def by_axis(value, axes):
    far, near = axes
    return taken_together(taken_together(value, near), far)


def together(arrays, axis):
    ravelled, at, outs = (jnp.concatenate([a.reshape(-1) for a in arrays]), 0, [])
    running = by_axis(ravelled, axis)
    for a in arrays:
        outs.append(running[at : at + a.size].reshape(a.shape))
        at += a.size
    return tuple(outs)


def contract_rows(left, right, precision):
    return lax.dot_general(
        left,
        right,
        (((0,), (0,)), ((), ())),
        precision=precision,
        preferred_element_type=jnp.float32,
    )


def on_device(
    saved_input,
    cot_inproj,
    cot_outproj,
    factor_inproj,
    factor_outproj,
    weight_inproj,
    weight_outproj,
    first_inproj,
    first_outproj,
    second_inproj,
    second_outproj,
):
    highest = lax.Precision.HIGHEST
    pieces = side_by_side((factor_inproj, factor_outproj), (("fs_0", "fs_1"), "fs_2"), 0, 1)
    mapped_in = jnp.dot(saved_input, pieces[0], preferred_element_type=jnp.float32)
    mapped_out = jnp.dot(saved_input, pieces[1], preferred_element_type=jnp.float32)
    term_in = contract_rows(mapped_in, cot_inproj.astype(jnp.float32), highest)
    term_out = contract_rows(mapped_out, cot_outproj.astype(jnp.float32), highest)
    projected_in, projected_out = sent_together(
        (term_in, term_out), (("fs_0", "fs_1"), "fs_2"), 0, 1
    )
    first_in_new = 0.8 * first_inproj + 0.2 * projected_in
    first_out_new = 0.8 * first_outproj + 0.2 * projected_out
    second_in_new = 0.9 * second_inproj + 0.1 * projected_in * projected_in
    second_out_new = 0.9 * second_outproj + 0.1 * projected_out * projected_out
    small_in = first_in_new / (jnp.sqrt(second_in_new) + 1e-08)
    small_out = first_out_new / (jnp.sqrt(second_out_new) + 1e-08)
    wide_in = factor_inproj.astype(jnp.float32)
    wide_out = factor_outproj.astype(jnp.float32)
    pieces = side_by_side((small_in, small_out), (("fs_0", "fs_1"), "fs_2"), 0, 1)
    full_in = jnp.dot(wide_in, pieces[0], precision=highest)
    full_out = jnp.dot(wide_out, pieces[1], precision=highest)
    square_in, square_out = together(
        (jnp.sum(full_in * full_in), jnp.sum(full_out * full_out)),
        (("fs_0", "fs_1"), ("fs_2", "tp")),
    )
    entries = float(full_in.shape[0] * full_in.shape[1] * lax.axis_size(FS) * lax.axis_size("tp"))
    update_in = full_in / jnp.sqrt(square_in / entries + 1e-06)
    update_out = full_out / jnp.sqrt(square_out / entries + 1e-06)
    fresh_in = weight_inproj - 0.02 * update_in
    fresh_out = weight_outproj - 0.02 * update_out
    copy_in, copy_out = side_by_side(
        (fresh_in.astype(jnp.bfloat16), fresh_out.astype(jnp.bfloat16)),
        (("fs_0", "fs_1"), "fs_2"),
        0,
        1,
    )
    return (
        update_in,
        update_out,
        fresh_in,
        fresh_out,
        copy_in,
        copy_out,
        first_in_new,
        first_out_new,
        second_in_new,
        second_out_new,
    )


def solution(mesh):
    finer = Mesh(mesh.devices.reshape(8, 8, 2, mesh.shape["tp"]), ("fs_0", "fs_1", "fs_2", "tp"))
    in_specs = (
        P(FS, None),
        P(FS, "tp"),
        P(FS, "tp"),
        P(FS, None),
        P(FS, None),
        P(FS, "tp"),
        P(FS, "tp"),
        P(FS, "tp"),
        P(FS, "tp"),
        P(FS, "tp"),
        P(FS, "tp"),
    )
    out_specs = (
        P(FS, "tp"),
        P(FS, "tp"),
        P(FS, "tp"),
        P(FS, "tp"),
        P(None, "tp"),
        P(None, "tp"),
        P(FS, "tp"),
        P(FS, "tp"),
        P(FS, "tp"),
        P(FS, "tp"),
    )
    return jax.shard_map(
        on_device, mesh=finer, in_specs=in_specs, out_specs=out_specs, check_vma=False
    )
```

profile of v0, /device:TPU:1, one launch (start us, length us, event | category | flops | bytes accessed | tf_op | source)
XLA Modules:
  0.0 193.0 jit_solution(12129395717456086654)
XLA Ops:
  0.7 0.9 pad_maximum_fusion.1
  1.6 44.4 %all_to_all.52 = bf16[64,16,512]{2,1,0:T(8,128)(2,1)S(1)} all-to-all(bf16[64,16,512]{2,1,0:T(8,128)(2,1)S(1)} %broadcast_in_dim.16), channel_id=1, replica_groups=mesh['fs_0'=8,'fs_1'=8,'fs_2'=2,'tp'=4] {'fs_0','fs_1'}, dimensions={0} | all-to-all | bytes 2097152 | tf_op jit(solution)/shard_map/all_to_all | solution.py:12
  46.3 8.3 %all_to_all.53 = bf16[2,64,16,512]{3,2,1,0:T(8,128)(2,1)S(1)} all-to-all(bf16[2,64,16,512]{3,2,1,0:T(8,128)(2,1)S(1)} %broadcast_in_dim.17), channel_id=1, replica_groups=mesh['fs_0'=8,'fs_1'=8,'fs_2'=2,'tp'=4] {'fs_2'}, dimensions={0} | all-to-all | bytes 4194304 | tf_op jit(solution)/shard_map/all_to_all | solution.py:12
  54.9 1.0 fusion
  55.9 1.0 fusion.2
  58.3 0.8 pad_maximum_fusion
  59.1 2.0 %copy.37 = f32[256,512]{1,0:T(8,128)} copy(f32[256,512]{0,1:T(8,128)} %pad_maximum_fusion) | data formatting | bytes 1048576 | tf_op jit(solution)/shard_map/concatenate | solution.py:57
  61.1 2.1 %reshape_reshape.13 = f32[64,2,2,512]{3,2,1,0:T(2,128)} reshape(f32[256,512]{1,0:T(8,128)} %copy.37) | data formatting | bytes 1048576 | tf_op jit(solution)/shard_map/reshape;reshape | solution.py:41
  63.3 1.1 copy.38
  64.4 4.9 %all_to_all.54 = f32[2,64,2,512]{3,2,1,0:T(2,128)} all-to-all(f32[2,64,2,512]{3,2,1,0:T(2,128)S(1)} %copy.38), channel_id=1, replica_groups=mesh['fs_0'=8,'fs_1'=8,'fs_2'=2,'tp'=4] {'fs_2'}, dimensions={0} | all-to-all | bytes 1048576 | tf_op jit(solution)/shard_map/all_to_all | solution.py:46
  69.3 2.1 %reduce_sum.54 = f32[64,2,512]{2,1,0:T(2,128)} reduce(f32[2,64,2,512]{3,2,1,0:T(2,128)} %all_to_all.54, f32[]{:T(128)} %constant.7.clone.1), dimensions={0}, to_apply=%region_0.0 | reduce | flops 65536 | bytes 786436 | tf_op jit(solution)/shard_map/reduce_sum | solution.py:47
  71.4 19.3 %all_to_all.55 = f32[64,2,512]{2,1,0:T(2,128)S(1)} all-to-all(f32[64,2,512]{2,1,0:T(2,128)} %reduce_sum.54), channel_id=1, replica_groups=mesh['fs_0'=8,'fs_1'=8,'fs_2'=2,'tp'=4] {'fs_0','fs_1'}, dimensions={0} | all-to-all | bytes 524288 | tf_op jit(solution)/shard_map/all_to_all | solution.py:53
  91.6 17.7 %all_to_all.56 = f32[64,2,512]{2,1,0:T(2,128)S(1)} all-to-all(f32[64,2,512]{2,1,0:T(2,128)S(1)} %broadcast_in_dim.18), channel_id=1, replica_groups=mesh['fs_0'=8,'fs_1'=8,'fs_2'=2,'tp'=4] {'fs_0','fs_1'}, dimensions={0} | all-to-all | bytes 524288 | tf_op jit(solution)/shard_map/all_to_all | solution.py:12
  109.4 7.3 %all_to_all.57 = f32[2,64,2,512]{3,2,1,0:T(2,128)S(1)} all-to-all(f32[2,64,2,512]{3,2,1,0:T(2,128)S(1)} %broadcast_in_dim.19), channel_id=1, replica_groups=mesh['fs_0'=8,'fs_1'=8,'fs_2'=2,'tp'=4] {'fs_2'}, dimensions={0} | all-to-all | bytes 1048576 | tf_op jit(solution)/shard_map/all_to_all | solution.py:12
  116.7 0.8 copy.40
  117.5 2.2 %reshape_reshape.14 = f32[256,512]{1,0:T(8,128)} reshape(f32[64,2,2,512]{3,2,1,0:T(2,128)} %copy.40) | data formatting | bytes 1048576 | tf_op jit(solution)/shard_map/reshape;reshape | solution.py:20
  119.7 1.8 multiply_reduce_fusion
  121.5 1.8 multiply_reduce_fusion.1
  123.3 1.4 pad_maximum_fusion.4
  124.7 9.1 %all_to_all.58 = f32[8,1,2]{2,1,0:T(1,128)S(1)} all-to-all(f32[8,1,2]{2,1,0:T(1,128)S(1)} %broadcast_in_dim.20), channel_id=1, replica_groups=mesh['fs_0'=8,'fs_1'=8,'fs_2'=2,'tp'=4] {'fs_2','tp'}, dimensions={0} | all-to-all | bytes 128 | tf_op jit(solution)/shard_map/all_to_all | solution.py:12
  133.8 14.7 %all_to_all.59 = f32[64,1,2]{2,1,0:T(1,128)S(1)} all-to-all(f32[64,1,2]{2,1,0:T(1,128)S(1)} %broadcast_in_dim.21), channel_id=1, replica_groups=mesh['fs_0'=8,'fs_1'=8,'fs_2'=2,'tp'=4] {'fs_0','fs_1'}, dimensions={0} | all-to-all | bytes 1024 | tf_op jit(solution)/shard_map/all_to_all | solution.py:12
  151.3 30.1 %all_to_all.60 = bf16[64,16,512]{2,1,0:T(8,128)(2,1)S(1)} all-to-all(bf16[64,16,512]{2,1,0:T(8,128)(2,1)S(1)} %broadcast_in_dim.22), channel_id=1, replica_groups=mesh['fs_0'=8,'fs_1'=8,'fs_2'=2,'tp'=4] {'fs_0','fs_1'}, dimensions={0} | all-to-all | bytes 2097152 | tf_op jit(solution)/shard_map/all_to_all | solution.py:12
  181.7 9.6 %all_to_all.61 = bf16[2,64,16,512]{3,2,1,0:T(8,128)(2,1)S(1)} all-to-all(bf16[2,64,16,512]{3,2,1,0:T(8,128)(2,1)S(1)} %broadcast_in_dim.23), channel_id=1, replica_groups=mesh['fs_0'=8,'fs_1'=8,'fs_2'=2,'tp'=4] {'fs_2'}, dimensions={0} | all-to-all | bytes 4194304 | tf_op jit(solution)/shard_map/all_to_all | solution.py:12
  191.5 1.5 fusion.14
  (42 shorter events, 4.9 us)
Async XLA Ops:
  0.6 54.2 %copy-start = (bf16[768,2048]{1,0:T(8,128)(2,1)S(1)}, bf16[768,2048]{1,0:T(8,128)(2,1)}, u32[]{:S(2)}) copy-start(bf16[768,2048]{1,0:T(8,128)(2,1)} %param.11) | copy-start | bytes 9437188
  55.9 1.1 copy-start.1
  55.9 1.7 copy-start.2
  63.3 27.6 %copy-start.7 = (f32[2,256]{1,0:T(2,128)S(1)}, f32[2,256]{1,0:T(2,128)}, u32[]{:S(2)}) copy-start(f32[2,256]{1,0:T(2,128)} %param.20) | copy-start | bytes 6148
  63.3 27.6 %copy-start.8 = (f32[2,256]{1,0:T(2,128)S(1)}, f32[2,256]{1,0:T(2,128)}, u32[]{:S(2)}) copy-start(f32[2,256]{1,0:T(2,128)} %param.18) | copy-start | bytes 6148
  63.3 27.6 %copy-start.9 = (f32[2,256]{1,0:T(2,128)S(1)}, f32[2,256]{1,0:T(2,128)}, u32[]{:S(2)}) copy-start(f32[2,256]{1,0:T(2,128)} %param.21) | copy-start | bytes 6148
  63.3 27.6 %copy-start.10 = (f32[2,256]{1,0:T(2,128)S(1)}, f32[2,256]{1,0:T(2,128)}, u32[]{:S(2)}) copy-start(f32[2,256]{1,0:T(2,128)} %param.19) | copy-start | bytes 6148
  109.3 10.5 %copy-start.3 = (bf16[16,256]{1,0:T(8,128)(2,1)S(1)}, bf16[16,256]{1,0:T(8,128)(2,1)}, u32[]{:S(2)}) copy-start(bf16[16,256]{1,0:T(8,128)(2,1)} %param.15) | copy-start | bytes 24580
  109.3 12.3 %copy-start.4 = (bf16[16,256]{1,0:T(8,128)(2,1)S(1)}, bf16[16,256]{1,0:T(8,128)(2,1)}, u32[]{:S(2)}) copy-start(bf16[16,256]{1,0:T(8,128)(2,1)} %param.14) | copy-start | bytes 24580
  109.4 41.1 %copy-start.5 = (f32[16,256]{1,0:T(8,128)S(1)}, f32[16,256]{1,0:T(8,128)}, u32[]{:S(2)}) copy-start(f32[16,256]{1,0:T(8,128)} %param.16) | copy-start | bytes 49156
  109.4 41.1 %copy-start.6 = (f32[16,256]{1,0:T(8,128)S(1)}, f32[16,256]{1,0:T(8,128)}, u32[]{:S(2)}) copy-start(f32[16,256]{1,0:T(8,128)} %param.17) | copy-start | bytes 49156
where the time goes:
time: 194 us; the launch traced here: 193 us
  blocking collectives  165 us (85%)
  local copies, waits for them, and re-layouts  11.9 us (6%)
  matrix products  6.89 us (4%)
  other arithmetic  6.64 us (3%)
  between operations  2.24 us (1%)
    all_to_all x8, blocking collectives, from_everyone(): lax.all_to_all(jnp.broadcast_to(value[None], (length, *value.shape)), axi...  141 us
    all_to_all x1, blocking collectives, sum_by_axis(): return jnp.sum(lax.all_to_all(own, far, 0, 0, tiled=True), axis=0)  19.3 us
    all_to_all x1, blocking collectives, summed_on_arrival(): lax.all_to_all(blocks, axis, split_axis=0, concat_axis=0, tiled=True)  4.88 us

commit v1 on v0

v1 whole, which is shorter than its diff:
```python
import functools

import jax
import jax.numpy as jnp
from jax import lax
from jax.experimental import pallas as pl
from jax.experimental.pallas import tpu as pltpu
from jax.sharding import PartitionSpec as P

MESH = pl.DeviceIdType.MESH
F32 = jnp.float32
BF16 = jnp.bfloat16
FAR_FIRST = (4, 3, 5, 2, 6, 1, 7)
NEAR_FIRST = (1, 7, 2, 6, 3, 5, 4)
ROWS_FIRST = (((0,), (0,)), ((), ()))


def rank_order():
    r = lax.broadcasted_iota(jnp.int32, (256, 256), 0)
    p = lax.broadcasted_iota(jnp.int32, (256, 256), 1)
    target = ((r >> 2) & 7) * 32 + (r >> 5) * 4 + (r & 3)
    return jnp.where(target == p, 1.0, 0.0).astype(BF16)


def halves(value):
    high = value.astype(BF16)
    return high, (value - high.astype(F32)).astype(BF16)


def kernel(
    entries,
    saved, cot_in, cot_out, f_in, f_out, w_in, w_out, m1_in, m1_out, m2_in, m2_out,
    upd_in, upd_out, new_in, new_out, copies, fst_in, fst_out, snd_in, snd_out,
    s_v, c_v, fl, ft, wl, r1_in, r1_out, r2_in, r2_out, mo, mg, m1c, m2c,
    fg, gh, gl, pp, prx, ps, rb, ab, sm, full, wg, qb, stage, arrived, nst, nrx,
    load_sem, a1_send, a1_recv, mo_send, mo_recv, w1_send, w1_recv, w2_send, w2_recv,
    a2_send, a2_recv, part_send, part_recv, b1_send, b1_recv, b2_send, b2_recv,
    b3_send, b3_recv, c_send, c_recv, q_send, q_recv, n_send, n_recv, o_send, o_recv,
    e_send, e_recv,
):
    me, x = lax.axis_index("fs"), lax.axis_index("tp")
    c = lax.rem(me, 2)
    y = lax.rem(lax.div(me, 2), 8)
    z = lax.div(me, 16)
    u = z + c * (y - z)
    v = y + c * (z - y)
    other = 1 - c

    def plus(at, k):
        return lax.rem(at + k % 8, 8)

    def dev(zz, yy, cc):
        return ((zz * 8 + yy) * 2 + cc, x)

    def along_u(k):
        to = plus(u, k)
        return dev(to + c * (v - to), v + c * (to - v), c)

    def along_v(k):
        to = plus(v, k)
        return dev(u + c * (to - u), to + c * (u - to), c)

    partner = dev(z, y, other)
    sent = []

    def send(src, dst, send_sem, recv_sem, device):
        copy = pltpu.make_async_remote_copy(
            src_ref=src, dst_ref=dst, send_sem=send_sem, recv_sem=recv_sem,
            device_id=device, device_id_type=MESH,
        )
        copy.start()
        sent.append(copy)

    def arrive(dst, recv_sem):
        pltpu.make_async_copy(dst, dst, recv_sem).wait()

    loads = {}

    def load(name, src, dst):
        loads[name] = pltpu.make_async_copy(src, dst, load_sem.at[len(loads)])
        loads[name].start()

    load("f_in", f_in, fl.at[0])
    load("f_out", f_out, ft)
    load("m1_in", m1_in, r1_in)
    load("m1_out", m1_out, r1_out)
    load("m2_in", m2_in, r2_in)
    load("m2_out", m2_out, r2_out)
    load("w_in", w_in, wl.at[0])
    load("w_out", w_out, wl.at[1])
    load("c_in", cot_in, c_v.at[:, 0:256])
    load("c_out", cot_out, c_v.at[:, 256:512])
    load("saved", saved, s_v)

    barrier = pltpu.get_barrier_semaphore()
    peers = [partner]
    for k in range(1, 8):
        for cc in range(2):
            peers.append(dev(plus(z, k), y, cc))
            peers.append(dev(z, plus(y, k), cc))
    for k in range(1, 4):
        peers.append((me, lax.rem(x + k, 4)))
    for peer in peers:
        pl.semaphore_signal(barrier, inc=1, device_id=peer, device_id_type=MESH)

    order = rank_order()
    for name in ("f_in", "f_out", "m1_in", "m1_out", "m2_in", "m2_out"):
        loads[name].wait()
    fl[1] = jnp.dot(ft[...], order, preferred_element_type=F32).astype(BF16)
    fg[c, v, u, c] = fl[c]
    mo[0, 0:2] = r1_in[...]
    mo[0, 2:4] = r2_in[...]
    mo[1, 0:2] = r1_out[...]
    mo[1, 2:4] = r2_out[...]
    mg[v, c] = mo[c]
    loads["w_in"].wait()
    loads["w_out"].wait()
    wg[v, u, c] = wl[c]
    pl.semaphore_wait(barrier, len(peers))

    def to_line(X, k):
        return dev(plus(z, k), y, 0) if X == 0 else dev(z, plus(y, k), 1)

    def to_cross(X, k):
        return dev(z, plus(y, k), 0) if X == 0 else dev(plus(z, k), y, 1)

    at_u, at_v = (z, y), (y, z)
    for k in FAR_FIRST:
        for X in range(2):
            send(fl.at[X], fg.at[X, at_v[X], at_u[X], c], a1_send.at[X, k], a1_recv.at[k, c], to_line(X, k))
    send(fl.at[other], fg.at[other, u, v, c], a1_send.at[0, 0], a1_recv.at[0, c], partner)
    for k in FAR_FIRST:
        for X in range(2):
            send(mo.at[X], mg.at[at_v[X], c], mo_send.at[X, k], mo_recv.at[k, c], to_cross(X, k))
    send(mo.at[other], mg.at[u, c], mo_send.at[0, 0], mo_recv.at[0, c], partner)
    for k in FAR_FIRST:
        for X in range(2):
            send(wl.at[X], wg.at[at_v[X], at_u[X], c], w1_send.at[X, k], w1_recv.at[k, c], to_line(X, k))
    send(wl.at[other], wg.at[u, v, c], w1_send.at[0, 0], w1_recv.at[0, c], partner)

    loads["c_in"].wait()
    loads["c_out"].wait()
    loads["saved"].wait()

    def grad(zc, carry):
        at = pl.ds(pl.multiple_of(zc * 256, 256), 256)
        g = lax.dot_general(s_v[:, at], c_v[...], ROWS_FIRST, preferred_element_type=F32)
        high, low = halves(g)
        high, low = high.reshape(8, 32, 512), low.reshape(8, 32, 512)
        gh[0, :, zc] = high[:, :, 0:256]
        gl[0, :, zc] = low[:, :, 0:256]
        gh[1, zc] = high[:, :, 256:512]
        gl[1, zc] = low[:, :, 256:512]
        return carry

    lax.fori_loop(0, 4, grad, 0)

    for k in NEAR_FIRST:
        for cc in range(2):
            arrive(fg.at[c, v, plus(u, -k), cc], a1_recv.at[k, cc])
    arrive(fg.at[c, v, u, other], a1_recv.at[0, other])

    def pass_on(j, part_k):
        at = fg.at[c, plus(v, j)]
        send(at, at, part_send.at[part_k], part_recv.at[part_k], partner)

    line = fg.at[c, v]
    for i, k in enumerate((2, -2, 1, -1)):
        send(line, line, a2_send.at[i], a2_recv.at[i], along_v(k))
    pass_on(0, 0)

    lax.fori_loop(4, 8, grad, 0)

    def project(X, j):
        f = fg[X, j].reshape(256, 256)
        term = lax.dot_general(f, gh[X, j].reshape(256, 256), ROWS_FIRST, preferred_element_type=F32)
        term += lax.dot_general(f, gl[X, j].reshape(256, 256), ROWS_FIRST, preferred_element_type=F32)
        return term.reshape(8, 32, 256)

    low, high = pl.ds(0, 4), pl.ds(4, 4)
    left, right = fg.at[c, plus(v, -2)], fg.at[c, plus(v, 2)]
    arrive(left, a2_recv.at[0])
    send(left, left, a2_send.at[4], a2_recv.at[4], along_v(1))
    send(left.at[low], left.at[low], a2_send.at[6], a2_recv.at[6], along_v(2))
    arrive(right, a2_recv.at[1])
    send(right, right, a2_send.at[5], a2_recv.at[5], along_v(-1))
    send(right.at[high], right.at[high], a2_send.at[7], a2_recv.at[7], along_v(-2))
    pass_on(-2, 1)
    pass_on(2, 2)
    arrive(fg.at[c, plus(v, -1)], a2_recv.at[2])
    pass_on(-1, 3)
    arrive(fg.at[c, plus(v, 1)], a2_recv.at[3])
    pass_on(1, 4)

    for k in NEAR_FIRST:
        for cc in range(2):
            arrive(wg.at[v, plus(u, -k), cc], w1_recv.at[k, cc])
    arrive(wg.at[v, u, other], w1_recv.at[0, other])

    def weight_step(s):
        a, b = plus(v, 1 - s), plus(v, s - 1)
        if s > 1:
            arrive(wg.at[a], w2_recv.at[0, s - 1])
            arrive(wg.at[b], w2_recv.at[1, s - 1])
        up, down = wg.at[a], wg.at[b]
        if s == 4:
            up, down = up.at[low], down.at[high]
        send(up, up, w2_send.at[0, s], w2_recv.at[0, s], along_v(1))
        send(down, down, w2_send.at[1, s], w2_recv.at[1, s], along_v(-1))

    weight_step(1)

    for k in NEAR_FIRST:
        for cc in range(2):
            arrive(mg.at[plus(v, -k), cc], mo_recv.at[k, cc])
    arrive(mg.at[v, other], mo_recv.at[0, other])
    for k in range(8):
        for cc in range(2):
            at = 4 * k + 2 * cc
            m1c[at:at + 2] = mg[k, cc, 0:2]
            m2c[at:at + 2] = mg[k, cc, 2:4]

    pp[c] = project(c, v)
    arrive(fg.at[other, u], part_recv.at[0])
    pp[other] = project(other, u)
    for j, part_k in ((-2, 1), (2, 2), (-1, 3), (1, 4)):
        pp[c] += project(c, plus(v, j))
        arrive(fg.at[other, plus(u, j)], part_recv.at[part_k])
        pp[other] += project(other, plus(u, j))
    arrive(fg.at[c, plus(v, -3)], a2_recv.at[4])
    pass_on(-3, 5)
    arrive(fg.at[c, plus(v, 3)], a2_recv.at[5])
    pass_on(3, 6)
    pp[c] += project(c, plus(v, -3))
    pp[c] += project(c, plus(v, 3))
    arrive(fg.at[c, plus(v, 4), low], a2_recv.at[6])
    arrive(fg.at[c, plus(v, 4), high], a2_recv.at[7])
    pass_on(4, 7)
    for j, part_k in ((-3, 5), (3, 6), (4, 7)):
        arrive(fg.at[other, plus(u, j)], part_recv.at[part_k])
        pp[other] += project(other, plus(u, j))

    for k in FAR_FIRST + (0,):
        at = plus(v, k)
        send(pp.at[other, at], prx.at[at], b1_send.at[k], b1_recv.at[k], partner)
    pp[c] += project(c, plus(v, 4))
    for k in FAR_FIRST + (0,):
        at = plus(u, k)
        arrive(prx.at[at], b1_recv.at[k])
        ps[at] = pp[c, at] + prx[at]
        if k:
            send(ps.at[at], rb.at[u], b2_send.at[k], b2_recv.at[k], along_u(k))
    weight_step(2)
    total = ps[u]
    for k in NEAR_FIRST:
        at = plus(u, -k)
        arrive(rb.at[at], b2_recv.at[k])
        total += rb[at]
    ab[v] = total

    for k in FAR_FIRST:
        send(ab.at[v], ab.at[v], b3_send.at[k], b3_recv.at[k], along_v(k))
    weight_step(3)
    for k in NEAR_FIRST:
        arrive(ab.at[plus(v, -k)], b3_recv.at[k])
    projected = ab[0]
    for k in range(1, 8):
        projected += ab[k]
    first = 0.8 * m1c[...] + 0.2 * projected
    second = 0.9 * m2c[...] + 0.1 * projected * projected
    sm[u] = first / (jnp.sqrt(second) + 1e-08)
    for k in FAR_FIRST:
        send(sm.at[u], sm.at[u], c_send.at[k], c_recv.at[k], along_u(k))
    weight_step(4)
    m1c[...] = first
    m2c[...] = second
    theirs = 4 * v + 2 * other
    for i in range(2):
        nst[i:i + 1] = m1c[pl.ds(theirs + i, 1)]
        nst[2 + i:3 + i] = m2c[pl.ds(theirs + i, 1)]
    send(nst, nrx, n_send, n_recv, partner)
    for k in NEAR_FIRST:
        arrive(sm.at[plus(u, -k)], c_recv.at[k])

    small_high, small_low = halves(sm[...].reshape(256, 256))

    def expand(j, squares):
        f = fg[c, j].reshape(256, 256)
        value = jnp.dot(f, small_high, preferred_element_type=F32)
        value += jnp.dot(f, small_low, preferred_element_type=F32)
        full[j] = value.reshape(8, 2, 16, 256)
        return squares + jnp.sum((value * value).reshape(32, 8, 256), axis=0)

    squares = lax.fori_loop(0, 8, expand, jnp.zeros((8, 256), F32))
    qb[x] = jnp.broadcast_to(jnp.sum(squares, keepdims=True), (8, 128))
    for k in (2, 1, 3):
        send(qb.at[x], qb.at[x], q_send.at[k], q_recv.at[k], (me, lax.rem(x + k, 4)))
    arrive(wg.at[plus(v, 4), low], w2_recv.at[0, 4])
    arrive(wg.at[plus(v, 4), high], w2_recv.at[1, 4])
    for k in (1, 3, 2):
        arrive(qb.at[lax.rem(x + 4 - k, 4)], q_recv.at[k])
    square = ((qb[0] + qb[1]) + qb[2]) + qb[3]
    scale = 1.0 / jnp.sqrt(square[0:1] / entries + 1e-06)
    scale = jnp.concatenate([scale, scale], axis=1)

    their_update = full[v, u, other] * scale
    stage[0] = their_update
    stage[1] = wg[v, u, other] - 0.02 * their_update
    send(stage, arrived, o_send, o_recv, partner)
    for j in range(8):
        update = full[j].reshape(256, 256) * scale
        fresh = wg[j].reshape(256, 256) - 0.02 * update
        copies[c, j] = fresh.astype(BF16).reshape(8, 32, 256)
        send(copies.at[c, j], copies.at[c, j], e_send.at[j], e_recv.at[j], partner)
    my_update = full[v, u, c] * scale
    my_new = wg[v, u, c] - 0.02 * my_update
    is_in = c == 0
    mine = 4 * v + 2 * c
    my_first = jnp.concatenate([m1c[pl.ds(mine, 1)], m1c[pl.ds(mine + 1, 1)]], axis=0)
    my_second = jnp.concatenate([m2c[pl.ds(mine, 1)], m2c[pl.ds(mine + 1, 1)]], axis=0)
    arrive(nrx, n_recv)
    fst_in[...] = jnp.where(is_in, my_first, nrx[0:2])
    fst_out[...] = jnp.where(is_in, nrx[0:2], my_first)
    snd_in[...] = jnp.where(is_in, my_second, nrx[2:4])
    snd_out[...] = jnp.where(is_in, nrx[2:4], my_second)
    arrive(arrived, o_recv)
    upd_in[...] = jnp.where(is_in, my_update, arrived[0])
    upd_out[...] = jnp.where(is_in, arrived[0], my_update)
    new_in[...] = jnp.where(is_in, my_new, arrived[1])
    new_out[...] = jnp.where(is_in, arrived[1], my_new)
    for j in range(8):
        arrive(copies.at[other, j], e_recv.at[j])
    for copy in sent:
        copy.wait_send()


def on_device(*args):
    shape = jax.ShapeDtypeStruct
    rows = shape((16, 256), F32)
    pair = shape((2, 256), F32)
    dma = pltpu.SemaphoreType.DMA
    vmem = pltpu.VMEM
    scratch = [
        vmem((768, 2048), BF16), vmem((768, 512), BF16),
        vmem((2, 16, 256), BF16), vmem((16, 256), BF16), vmem((2, 16, 256), F32),
        vmem((2, 256), F32), vmem((2, 256), F32), vmem((2, 256), F32), vmem((2, 256), F32),
        vmem((2, 8, 256), F32), vmem((8, 2, 8, 256), F32),
        vmem((32, 256), F32), vmem((32, 256), F32),
        vmem((2, 8, 8, 2, 16, 256), BF16),
        vmem((2, 8, 8, 32, 256), BF16), vmem((2, 8, 8, 32, 256), BF16),
        vmem((2, 8, 32, 256), F32), vmem((8, 32, 256), F32), vmem((8, 32, 256), F32),
        vmem((8, 32, 256), F32), vmem((8, 32, 256), F32), vmem((8, 32, 256), F32),
        vmem((8, 8, 2, 16, 256), F32), vmem((8, 8, 2, 16, 256), F32),
        vmem((4, 8, 128), F32), vmem((2, 16, 256), F32), vmem((2, 16, 256), F32),
        vmem((8, 256), F32), vmem((8, 256), F32),
        dma((11,)),
        dma((2, 8)), dma((8, 2)), dma((2, 8)), dma((8, 2)), dma((2, 8)), dma((8, 2)),
        dma((2, 5)), dma((2, 5)),
        dma((8,)), dma((8,)), dma((8,)), dma((8,)), dma((8,)), dma((8,)),
        dma((8,)), dma((8,)), dma((8,)), dma((8,)), dma((8,)), dma((8,)),
        dma((4,)), dma((4,)), dma, dma, dma, dma, dma((8,)), dma((8,)),
    ]
    scratch = [s(()) if s is dma else s for s in scratch]
    upd_in, upd_out, new_in, new_out, copies, fst_in, fst_out, snd_in, snd_out = pl.pallas_call(
        functools.partial(kernel, float(2048 * 1024)),
        out_shape=(rows, rows, rows, rows, shape((2, 8, 8, 32, 256), BF16), pair, pair, pair, pair),
        in_specs=[pl.BlockSpec(memory_space=pl.ANY)] * 11,
        out_specs=(pl.BlockSpec(memory_space=pltpu.VMEM),) * 9,
        scratch_shapes=scratch,
        compiler_params=pltpu.CompilerParams(collective_id=0, has_side_effects=True),
    )(*args)
    copy_in = jnp.swapaxes(copies[0], 0, 1).reshape(2048, 256)
    copy_out = copies[1].reshape(2048, 256)
    return (upd_in, upd_out, new_in, new_out, copy_in, copy_out, fst_in, fst_out, snd_in, snd_out)


def solution(mesh):
    both, rows, columns = P("fs", "tp"), P("fs", None), P(None, "tp")
    return jax.shard_map(
        on_device,
        mesh=mesh,
        in_specs=(rows, both, both, rows, rows) + (both,) * 6,
        out_specs=(both,) * 4 + (columns,) * 2 + (both,) * 4,
        check_vma=False,
    )
```

time: 194 us -> 77 us (0.40)
  blocking collectives: 165 us -> 0 us
  Pallas kernels: 0 us -> 67.7 us
  matrix products: 6.89 us -> 0 us
  other arithmetic: 6.64 us -> 0 us
  local copies, waits for them, and re-layouts: 11.9 us -> 8.49 us
    all_to_all x10 -> x0, blocking collectives: 165 us -> none  [the longest x8 141 us: from_everyone(): lax.all_to_all(jnp.broadcast_to(value[None], (length, *value.shape)), axi...]
    pallas_call x0 -> x1, Pallas kernels: none -> 67.7 us  [on_device(): pl.pallas_call(functools.partial(kernel, float(2048 * 1024)), out_shape=(...]
    dot_general x6 -> x0, matrix products: 6.89 us -> none  [the longest x1 1.78 us: on_device(): full_out = jnp.dot(wide_out, pieces[1], precision=highest)]
    unnamed x22 -> x24, local copies, waits for them, and re-layouts: 0.06 us -> 4.76 us
    another operation x2 -> x0, local copies, waits for them, and re-layouts: 4.33 us -> none  [the longest x1 2.19 us: in_order(): return jnp.moveaxis(blocks, 0, dim).reshape(dims)]
    concatenate x5 -> x0, other arithmetic: 3.07 us -> none  [the longest x1 1.37 us: together(): jnp.concatenate([a.reshape(-1) for a in arrays])]
    reduce_sum x4 -> x0, other arithmetic: 2.34 us -> none  [the longest x1 2.12 us: summed_on_arrival(): return arrived.sum(axis=0)]
    slice x1, local copies, waits for them, and re-layouts: 0.59 us -> 2.68 us  [on_device(): copy_out = copies[1].reshape(2048, 256)]
where the time goes in v1:
time: 77 us; the launch traced here: 76.9 us
  Pallas kernels  67.7 us (88%)
  local copies, waits for them, and re-layouts  8.49 us (11%)
    pallas_call x1, Pallas kernels, on_device(): pl.pallas_call(functools.partial(kernel, float(2048 * 1024)), out_shape=(...  67.7 us
    unnamed x24, local copies, waits for them, and re-layouts  4.76 us
    slice x1, local copies, waits for them, and re-layouts, on_device(): copy_out = copies[1].reshape(2048, 256)  2.68 us

profile of v1, /device:TPU:1, one launch (start us, length us, event | category | flops | bytes accessed | tf_op | source)
XLA Modules:
  0.0 76.9 jit_solution(15751633115443925285)
XLA Ops:
  0.6 67.7 %shard_map.186 = (f32[16,256]{1,0:T(8,128)}, f32[16,256]{1,0:T(8,128)}, f32[16,256]{1,0:T(8,128)}, f32[16,256]{1,0:T(8,128)}, bf16[2,8,8,32,256]{4,3,2,1,0:T(8,1...) custom-call(bf16[768,2048]{1,0:T(8,128)(2,1)} %saved.1, ...), custom_call_target="tpu_custom_call" | custom-call | tf_op jit(solution)/shard_map/pallas_call | solution.py:364
  68.3 2.7 %fusion = (bf16[1,8,8,32,256]{4,3,2,1,0:T(8,128)(2,1)}, bf16[8,8,32,256]{3,2,0,1:T(8,128)(2,1)S(1)}) fusion(bf16[2,8,8,32,256]{4,3,2,1,0:T(8,128)(2,1)} %get-tuple-element.23), kind=kLoop, calls=%fused_computation.1 | loop fusion | bytes 4194304 | tf_op jit(solution)/shard_map/slice | solution.py:373
  71.0 0.0 copy-start.3
  71.0 0.0 copy-start.7
  71.0 0.0 copy-start.6
  71.0 0.0 copy-start.5
  71.1 0.0 copy-start.4
  71.1 1.0 %copy.21 = bf16[8,8,32,256]{3,2,1,0:T(8,128)(2,1)} copy(bf16[8,8,32,256]{3,2,0,1:T(8,128)(2,1)S(1)} %get-tuple-element.29) | data formatting | bytes 2097152 | tf_op jit(solution)/shard_map/transpose | solution.py:372
  72.1 0.0 copy-done.3
  72.1 0.6 copy.30
  72.7 0.0 copy-done.2
  72.7 0.6 copy.31
  73.3 0.0 copy-done.1
  73.3 0.6 copy.32
  73.9 0.0 copy-done
  73.9 0.6 copy.33
  74.5 0.0 copy-done.7
  74.5 0.6 copy.34
  75.1 0.0 copy-done.6
  75.1 0.6 copy.35
  75.7 0.0 copy-done.5
  75.7 0.6 copy.36
  76.3 0.0 copy-done.4
  76.3 0.6 copy.37
  (3 shorter events, 0.0 us)
Async XLA Ops:
  71.0 1.1 %copy-start.3 = (f32[16,256]{1,0:T(8,128)S(1)}, f32[16,256]{1,0:T(8,128)}, u32[]{:S(2)}) copy-start(f32[16,256]{1,0:T(8,128)} %get-tuple-element.40) | copy-start | bytes 49156
  71.0 1.7 %copy-start.2 = (f32[16,256]{1,0:T(8,128)S(1)}, f32[16,256]{1,0:T(8,128)}, u32[]{:S(2)}) copy-start(f32[16,256]{1,0:T(8,128)} %get-tuple-element.41) | copy-start | bytes 49156
  71.0 2.3 %copy-start.1 = (f32[16,256]{1,0:T(8,128)S(1)}, f32[16,256]{1,0:T(8,128)}, u32[]{:S(2)}) copy-start(f32[16,256]{1,0:T(8,128)} %get-tuple-element.42) | copy-start | bytes 49156
  71.0 2.9 %copy-start = (f32[16,256]{1,0:T(8,128)S(1)}, f32[16,256]{1,0:T(8,128)}, u32[]{:S(2)}) copy-start(f32[16,256]{1,0:T(8,128)} %get-tuple-element.43) | copy-start | bytes 49156
  71.0 3.5 %copy-start.7 = (f32[2,256]{1,0:T(2,128)S(1)}, f32[2,256]{1,0:T(2,128)}, u32[]{:S(2)}) copy-start(f32[2,256]{1,0:T(2,128)} %get-tuple-element.46) | copy-start | bytes 6148
  71.0 4.1 %copy-start.6 = (f32[2,256]{1,0:T(2,128)S(1)}, f32[2,256]{1,0:T(2,128)}, u32[]{:S(2)}) copy-start(f32[2,256]{1,0:T(2,128)} %get-tuple-element.47) | copy-start | bytes 6148
  71.0 4.7 %copy-start.5 = (f32[2,256]{1,0:T(2,128)S(1)}, f32[2,256]{1,0:T(2,128)}, u32[]{:S(2)}) copy-start(f32[2,256]{1,0:T(2,128)} %get-tuple-element.48) | copy-start | bytes 6148
  71.1 5.2 %copy-start.4 = (f32[2,256]{1,0:T(2,128)S(1)}, f32[2,256]{1,0:T(2,128)}, u32[]{:S(2)}) copy-start(f32[2,256]{1,0:T(2,128)} %get-tuple-element.49) | copy-start | bytes 6148

commit v2 on v1

v2 whole, which is shorter than its diff:
```python
import functools

import jax
import jax.numpy as jnp
from jax import lax
from jax.experimental import pallas as pl
from jax.experimental.pallas import tpu as pltpu
from jax.sharding import PartitionSpec as P

MESH = pl.DeviceIdType.MESH
F32 = jnp.float32
BF16 = jnp.bfloat16
FAR_FIRST = (4, 3, 5, 2, 6, 1, 7)
NEAR_FIRST = (1, 7, 2, 6, 3, 5, 4)
ROWS_FIRST = (((0,), (0,)), ((), ()))


def rank_order():
    r = lax.broadcasted_iota(jnp.int32, (256, 256), 0)
    p = lax.broadcasted_iota(jnp.int32, (256, 256), 1)
    target = ((r >> 2) & 7) * 32 + (r >> 5) * 4 + (r & 3)
    return jnp.where(target == p, 1.0, 0.0).astype(BF16)


def halves(value):
    high = value.astype(BF16)
    return high, (value - high.astype(F32)).astype(BF16)


def kernel(
    entries,
    saved, cot_in, cot_out, f_in, f_out, w_in, w_out, m1_in, m1_out, m2_in, m2_out,
    copies, rows, moments,
    s_v, c_v, fl, ft, wl, r1_in, r1_out, r2_in, r2_out, mo, mg, m1c, m2c,
    fg, go, gs, gr, gh, gl, pp, rb, ab, sm, full, wg, qb, nst, nrx,
    load_sem, a1_send, a1_recv, mo_send, mo_recv, w1_send, w1_recv, w2_send, w2_recv,
    near_send, near_recv, two_recv, three_send, three_recv, four_send, four_recv,
    fp_send, fp_recv, wp_send, wp_recv, g_send, g_recv, b2_send, b2_recv,
    b3_send, b3_recv, c_send, c_recv, sp_send, sp_recv, q_send, q_recv, n_send, n_recv,
):
    me, x = lax.axis_index("fs"), lax.axis_index("tp")
    c = lax.rem(me, 2)
    y = lax.rem(lax.div(me, 2), 8)
    z = lax.div(me, 16)
    u = z + c * (y - z)
    v = y + c * (z - y)
    other = 1 - c

    def plus(at, k):
        return lax.rem(at + k % 8, 8)

    def dev(zz, yy, cc):
        return ((zz * 8 + yy) * 2 + cc, x)

    def along_u(k):
        to = plus(u, k)
        return dev(to + c * (v - to), v + c * (to - v), c)

    def along_v(k):
        to = plus(v, k)
        return dev(u + c * (to - u), to + c * (u - to), c)

    partner = dev(z, y, other)
    sent = []

    def send(src, dst, send_sem, recv_sem, device, later=True):
        copy = pltpu.make_async_remote_copy(
            src_ref=src, dst_ref=dst, send_sem=send_sem, recv_sem=recv_sem,
            device_id=device, device_id_type=MESH,
        )
        copy.start()
        if later:
            sent.append(copy)

    def arrive(dst, sem):
        pltpu.make_async_copy(dst, dst, sem).wait()

    loads = {}

    def load(name, src, dst):
        loads[name] = pltpu.make_async_copy(src, dst, load_sem.at[len(loads)])
        loads[name].start()

    load("f_in", f_in, fl.at[0])
    load("f_out", f_out, ft)
    load("m1_in", m1_in, r1_in)
    load("m1_out", m1_out, r1_out)
    load("m2_in", m2_in, r2_in)
    load("m2_out", m2_out, r2_out)
    load("w_in", w_in, wl.at[0])
    load("w_out", w_out, wl.at[1])
    load("c_in", cot_in, c_v.at[:, pl.ds(pl.multiple_of(256 * c, 256), 256)])
    load("c_out", cot_out, c_v.at[:, pl.ds(pl.multiple_of(256 * other, 256), 256)])
    load("saved", saved, s_v)

    barrier = pltpu.get_barrier_semaphore()
    peers = [partner]
    for k in range(1, 8):
        for cc in range(2):
            peers.append(dev(plus(z, k), y, cc))
            peers.append(dev(z, plus(y, k), cc))
    for k in range(1, 4):
        peers.append((me, lax.rem(x + k, 4)))
        peers.append((me + 1 - 2 * c, lax.rem(x + k, 4)))
    for peer in peers:
        pl.semaphore_signal(barrier, inc=1, device_id=peer, device_id_type=MESH)

    order = rank_order()
    for name in ("f_in", "f_out", "m1_in", "m1_out", "m2_in", "m2_out"):
        loads[name].wait()
    fl[1] = jnp.dot(ft[...], order, preferred_element_type=F32).astype(BF16)
    fg[c, v, u, c] = fl[c]
    mo[0, 0:2] = r1_in[...]
    mo[0, 2:4] = r2_in[...]
    mo[1, 0:2] = r1_out[...]
    mo[1, 2:4] = r2_out[...]
    mg[v, c] = mo[c]
    loads["w_in"].wait()
    loads["w_out"].wait()
    wg[c, v, u, c] = wl[c]
    pl.semaphore_wait(barrier, len(peers))

    def to_line(X, k):
        return dev(plus(z, k), y, 0) if X == 0 else dev(z, plus(y, k), 1)

    def to_cross(X, k):
        return dev(z, plus(y, k), 0) if X == 0 else dev(plus(z, k), y, 1)

    at_u, at_v = (z, y), (y, z)
    send(fl.at[other], fg.at[other, u, v, c], a1_send.at[0, 0], a1_recv.at[0, c], partner)
    for k in FAR_FIRST:
        for X in range(2):
            send(fl.at[X], fg.at[X, at_v[X], at_u[X], c], a1_send.at[X, k], a1_recv.at[k, c], to_line(X, k))

    def spread(k):
        block = fg.at[c, v, plus(u, -k)]
        if k:
            arrive(fg.at[c, v, plus(u, -k), 0], a1_recv.at[k, 0])
            arrive(fg.at[c, v, plus(u, -k), 1], a1_recv.at[k, 1])
        else:
            arrive(fg.at[c, v, u, other], a1_recv.at[0, other])
        send(block, block, near_send.at[0], two_recv.at[0, k], along_v(2), later=False)
        send(block, block, near_send.at[1], two_recv.at[1, k], along_v(-2), later=False)
        send(block, block, near_send.at[2], near_recv.at[0], along_v(1), later=False)
        send(block, block, near_send.at[3], near_recv.at[1], along_v(-1), later=False)

    spread(0)
    for k in FAR_FIRST:
        for X in range(2):
            send(wl.at[X], wg.at[X, at_v[X], at_u[X], c], w1_send.at[X, k], w1_recv.at[k, c], to_line(X, k))
    send(wl.at[other], wg.at[other, u, v, c], w1_send.at[0, 0], w1_recv.at[0, c], partner)

    loads["c_in"].wait()
    loads["c_out"].wait()
    loads["saved"].wait()

    def grad_copy(zc):
        return pltpu.make_async_remote_copy(
            src_ref=gs.at[zc], dst_ref=gr.at[zc], send_sem=g_send.at[zc], recv_sem=g_recv.at[zc],
            device_id=partner, device_id_type=MESH,
        )

    def grad(zc, carry):
        at = pl.ds(pl.multiple_of(zc * 256, 256), 256)
        g = lax.dot_general(s_v[:, at], c_v[...], ROWS_FIRST, preferred_element_type=F32)
        gs[zc] = g[:, 256:512]
        go[zc] = g[:, 0:256]
        grad_copy(zc).start()
        return carry

    lax.fori_loop(0, 4, grad, 0)

    for k in NEAR_FIRST:
        spread(k)

    for k in FAR_FIRST:
        for X in range(2):
            send(mo.at[X], mg.at[at_v[X], c], mo_send.at[X, k], mo_recv.at[k, c], to_cross(X, k))
    send(mo.at[other], mg.at[u, c], mo_send.at[0, 0], mo_recv.at[0, c], partner)
    lax.fori_loop(4, 8, grad, 0)

    for i, k in enumerate((0,) + NEAR_FIRST):
        left, right = fg.at[c, plus(v, -2), plus(u, -k)], fg.at[c, plus(v, 2), plus(u, -k)]
        arrive(left, two_recv.at[0, k])
        send(left, left, three_send.at[0], three_recv.at[0], along_v(1), later=False)
        if i % 2:
            send(left, left, four_send.at[k], four_recv.at[k], along_v(2))
        arrive(right, two_recv.at[1, k])
        send(right, right, three_send.at[1], three_recv.at[1], along_v(-1), later=False)
        if i % 2 == 0:
            send(right, right, four_send.at[k], four_recv.at[k], along_v(-2))
    half = (pl.ds(0, 4), pl.ds(4, 4))

    def pass_weight(j, i):
        at = wg.at[c, plus(v, j)]
        send(at, at, wp_send.at[i], wp_recv.at[i], partner)

    def weight_step(s):
        a, b = plus(v, 1 - s), plus(v, s - 1)
        up, down = wg.at[c, a], wg.at[c, b]
        if s > 1:
            arrive(up, w2_recv.at[0, s - 1])
            arrive(down, w2_recv.at[1, s - 1])
        if s == 4:
            up, down = up.at[half[0]], down.at[half[1]]
        send(up, up, w2_send.at[0, s], w2_recv.at[0, s], along_v(1))
        send(down, down, w2_send.at[1, s], w2_recv.at[1, s], along_v(-1))
        if s == 1:
            pass_weight(0, 0)
        else:
            pass_weight(1 - s, 2 * s - 3)
            pass_weight(s - 1, 2 * s - 2)

    for k in NEAR_FIRST:
        for cc in range(2):
            arrive(wg.at[c, v, plus(u, -k), cc], w1_recv.at[k, cc])
    arrive(wg.at[c, v, u, other], w1_recv.at[0, other])
    weight_step(1)
    def combine(zc, carry):
        pltpu.make_async_copy(gr.at[zc], gr.at[zc], g_recv.at[zc]).wait()
        high, low = halves(go[zc] + gr[zc])
        for i in range(8):
            a, b = i + c * (zc - i), zc + c * (i - zc)
            gh[a, b] = high[32 * i:32 * i + 32]
            gl[a, b] = low[32 * i:32 * i + 32]
        return carry

    lax.fori_loop(0, 8, combine, 0)

    def project(j):
        f = fg[c, j].reshape(256, 256)
        term = lax.dot_general(f, gh[j].reshape(256, 256), ROWS_FIRST, preferred_element_type=F32)
        term += lax.dot_general(f, gl[j].reshape(256, 256), ROWS_FIRST, preferred_element_type=F32)
        return term.reshape(8, 32, 256)

    def pass_factor(j, i):
        at = fg.at[c, plus(v, j)]
        send(at, at, fp_send.at[i], fp_recv.at[i], partner)

    pass_factor(0, 0)
    pass_factor(-2, 1)
    pass_factor(2, 2)
    pp[...] = project(v)
    pp[...] += project(plus(v, -2))
    pp[...] += project(plus(v, 2))
    arrive(fg.at[c, plus(v, -1)], near_recv.at[0])
    pp[...] += project(plus(v, -1))
    arrive(fg.at[c, plus(v, 1)], near_recv.at[1])
    pp[...] += project(plus(v, 1))
    pass_factor(-1, 3)
    pass_factor(1, 4)
    arrive(fg.at[c, plus(v, -3)], three_recv.at[0])
    pp[...] += project(plus(v, -3))
    arrive(fg.at[c, plus(v, 3)], three_recv.at[1])
    pp[...] += project(plus(v, 3))
    for k in (0,) + NEAR_FIRST:
        arrive(fg.at[c, plus(v, 4), plus(u, -k)], four_recv.at[k])
    pp[...] += project(plus(v, 4))
    for k in FAR_FIRST:
        send(pp.at[plus(u, k)], rb.at[u], b2_send.at[k], b2_recv.at[k], along_u(k))
    pass_factor(-3, 5)
    pass_factor(3, 6)
    pass_factor(4, 7)

    for k in NEAR_FIRST:
        for cc in range(2):
            arrive(mg.at[plus(v, -k), cc], mo_recv.at[k, cc])
    arrive(mg.at[v, other], mo_recv.at[0, other])
    for k in range(8):
        for cc in range(2):
            at = 4 * k + 2 * cc
            m1c[at:at + 2] = mg[k, cc, 0:2]
            m2c[at:at + 2] = mg[k, cc, 2:4]

    weight_step(2)
    total = pp[u]
    for k in NEAR_FIRST:
        at = plus(u, -k)
        arrive(rb.at[at], b2_recv.at[k])
        total += rb[at]
    ab[v] = total

    for k in FAR_FIRST:
        send(ab.at[v], ab.at[v], b3_send.at[k], b3_recv.at[k], along_v(k))
    weight_step(3)
    for k in NEAR_FIRST:
        arrive(ab.at[plus(v, -k)], b3_recv.at[k])
    projected = ab[0]
    for k in range(1, 8):
        projected += ab[k]
    first = 0.8 * m1c[...] + 0.2 * projected
    second = 0.9 * m2c[...] + 0.1 * projected * projected
    sm[c, u] = first / (jnp.sqrt(second) + 1e-08)
    for k in FAR_FIRST:
        send(sm.at[c, u], sm.at[c, u], c_send.at[k], c_recv.at[k], along_u(k))
    send(sm.at[c, u], sm.at[c, u], sp_send.at[0], sp_recv.at[0], partner)
    m1c[...] = first
    m2c[...] = second
    theirs = 4 * v + 2 * other
    for i in range(2):
        nst[i:i + 1] = m1c[pl.ds(theirs + i, 1)]
        nst[2 + i:3 + i] = m2c[pl.ds(theirs + i, 1)]
    send(nst, nrx, n_send, n_recv, partner)
    weight_step(4)
    for k in NEAR_FIRST:
        at = sm.at[c, plus(u, -k)]
        arrive(at, c_recv.at[k])
        send(at, at, sp_send.at[k], sp_recv.at[k], partner)

    def expanded(X):
        high, low = halves(sm[X].reshape(256, 256))
        small = jnp.concatenate([high, low], axis=0)

        def expand(j, squares):
            f = fg[X, j].reshape(256, 256)
            value = jnp.dot(jnp.concatenate([f, f], axis=1), small, preferred_element_type=F32)
            full[X, j] = value.reshape(8, 2, 16, 256)
            return squares + jnp.sum((value * value).reshape(32, 8, 256), axis=0)

        return lax.fori_loop(0, 8, expand, jnp.zeros((8, 256), F32), unroll=2)

    squares = expanded(c)
    qb[c, x] = jnp.broadcast_to(jnp.sum(squares, keepdims=True), (8, 128))
    mine = qb.at[c, x]
    for k in (2, 1, 3):
        to = lax.rem(x + k, 4)
        send(mine, mine, q_send.at[k, 0], q_recv.at[k, 0], (me, to))
        send(mine, mine, q_send.at[k, 1], q_recv.at[k, 1], (me + 1 - 2 * c, to))
    send(mine, mine, q_send.at[0, 1], q_recv.at[0, 1], partner)
    four = wg.at[c, plus(v, 4)]
    arrive(four.at[half[0]], w2_recv.at[0, 4])
    arrive(four.at[half[1]], w2_recv.at[1, 4])
    pass_weight(4, 7)
    for j, i in ((0, 0), (-2, 1), (2, 2), (-1, 3), (1, 4), (-3, 5), (3, 6), (4, 7)):
        arrive(fg.at[other, plus(u, j)], fp_recv.at[i])
    for k in (0,) + NEAR_FIRST:
        arrive(sm.at[other, plus(v, -k)], sp_recv.at[k])
    expanded(other)
    for k in (1, 3, 2):
        arrive(qb.at[c, lax.rem(x + 4 - k, 4)], q_recv.at[k, 0])
        arrive(qb.at[other, lax.rem(x + 4 - k, 4)], q_recv.at[k, 1])
    arrive(qb.at[other, x], q_recv.at[0, 1])

    def scale_of(X):
        square = ((qb[X, 0] + qb[X, 1]) + qb[X, 2]) + qb[X, 3]
        scale = 1.0 / jnp.sqrt(square[0:1] / entries + 1e-06)
        return jnp.concatenate([scale, scale], axis=1)

    def finish(X, first_line, last_line):
        scale = scale_of(X)

        def line(j, carry):
            update = full[X, j].reshape(256, 256) * scale
            fresh = wg[X, j].reshape(256, 256) - 0.02 * update
            rounded = fresh.astype(BF16)
            for i in range(8):
                copies[X, i + X * (j - i), j + X * (i - j)] = rounded[32 * i:32 * i + 32]
            return carry

        lax.fori_loop(first_line, last_line, line, 0)

    finish(c, 0, 8)
    for X in range(2):
        update = full[X, at_v[X], at_u[X], c] * scale_of(X)
        rows[X] = update
        rows[2 + X] = wl[X] - 0.02 * update
    own = 4 * v + 2 * c
    my_first = jnp.concatenate([m1c[pl.ds(own, 1)], m1c[pl.ds(own + 1, 1)]], axis=0)
    my_second = jnp.concatenate([m2c[pl.ds(own, 1)], m2c[pl.ds(own + 1, 1)]], axis=0)
    arrive(nrx, n_recv)
    is_in = c == 0
    moments[0] = jnp.where(is_in, my_first, nrx[0:2])
    moments[1] = jnp.where(is_in, nrx[0:2], my_first)
    moments[2] = jnp.where(is_in, my_second, nrx[2:4])
    moments[3] = jnp.where(is_in, nrx[2:4], my_second)
    for j, i in ((0, 0), (-1, 1), (1, 2), (-2, 3), (2, 4), (-3, 5), (3, 6), (4, 7)):
        arrive(wg.at[other, plus(u, j)], wp_recv.at[i])
    finish(other, 0, 8)
    for copy in sent:
        copy.wait_send()
    for i in range(4):
        arrive(fg.at[c, v], near_send.at[i])
    arrive(fg.at[c, v], three_send.at[0])
    arrive(fg.at[c, v], three_send.at[1])

    def drained(zc, carry):
        grad_copy(zc).wait_send()
        return carry

    lax.fori_loop(0, 8, drained, 0)


def write_out(copies, rows, moments, *refs):
    outs, sems = refs[:-1], refs[-1]
    sources = [copies.at[0], copies.at[1]] + [rows.at[i] for i in range(4)] + [moments.at[i] for i in range(4)]
    writes = [pltpu.make_async_copy(src, dst, sems.at[i]) for i, (src, dst) in enumerate(zip(sources, outs))]
    for write in writes:
        write.start()
    for write in writes:
        write.wait()


def on_device(*args):
    shape = jax.ShapeDtypeStruct
    dma = pltpu.SemaphoreType.DMA
    vmem = pltpu.VMEM
    anywhere = pl.BlockSpec(memory_space=pl.ANY)
    scratch = [
        vmem((768, 2048), BF16), vmem((768, 512), BF16),
        vmem((2, 16, 256), BF16), vmem((16, 256), BF16), vmem((2, 16, 256), F32),
        vmem((2, 256), F32), vmem((2, 256), F32), vmem((2, 256), F32), vmem((2, 256), F32),
        vmem((2, 8, 256), F32), vmem((8, 2, 8, 256), F32),
        vmem((32, 256), F32), vmem((32, 256), F32),
        vmem((2, 8, 8, 2, 16, 256), BF16),
        vmem((8, 256, 256), F32), vmem((8, 256, 256), F32), vmem((8, 256, 256), F32),
        vmem((8, 8, 32, 256), BF16), vmem((8, 8, 32, 256), BF16),
        vmem((8, 32, 256), F32), vmem((8, 32, 256), F32),
        vmem((8, 32, 256), F32), vmem((2, 8, 32, 256), F32),
        vmem((2, 8, 8, 2, 16, 256), F32), vmem((2, 8, 8, 2, 16, 256), F32),
        vmem((2, 4, 8, 128), F32), vmem((8, 256), F32), vmem((8, 256), F32),
        dma((11,)),
        dma((2, 8)), dma((8, 2)), dma((2, 8)), dma((8, 2)), dma((2, 8)), dma((8, 2)),
        dma((2, 5)), dma((2, 5)),
        dma((4,)), dma((2,)), dma((2, 8)), dma((2,)), dma((2,)), dma((8,)), dma((8,)),
        dma((8,)), dma((8,)), dma((8,)), dma((8,)), dma((8,)), dma((8,)), dma((8,)), dma((8,)),
        dma((8,)), dma((8,)), dma((8,)), dma((8,)), dma((8,)), dma((8,)), dma((4, 2)), dma((4, 2)),
        dma(()), dma(()),
    ]
    mid = pl.pallas_call(
        functools.partial(kernel, float(2048 * 1024)),
        out_shape=(shape((2, 8, 8, 32, 256), BF16), shape((4, 16, 256), F32), shape((4, 2, 256), F32)),
        in_specs=[pl.BlockSpec(memory_space=pltpu.HBM)] * 11,
        out_specs=(pl.BlockSpec(memory_space=pltpu.VMEM),) * 3,
        scratch_shapes=scratch,
        compiler_params=pltpu.CompilerParams(
            collective_id=0, has_side_effects=True, vmem_limit_bytes=40 * 1024 * 1024
        ),
    )(*(pltpu.with_memory_space_constraint(a, pltpu.HBM) for a in args))
    mid = [pltpu.with_memory_space_constraint(m, pltpu.VMEM) for m in mid]
    whole, row, pair = shape((8, 8, 32, 256), BF16), shape((16, 256), F32), shape((2, 256), F32)
    copy_in, copy_out, *rest = pl.pallas_call(
        write_out,
        out_shape=(whole, whole) + (row,) * 4 + (pair,) * 4,
        in_specs=[pl.BlockSpec(memory_space=pltpu.VMEM)] * 3,
        out_specs=(anywhere,) * 10,
        scratch_shapes=[dma((10,))],
    )(*mid)
    return (*rest[:4], copy_in.reshape(2048, 256), copy_out.reshape(2048, 256), *rest[4:])


def solution(mesh):
    both, rows, columns = P("fs", "tp"), P("fs", None), P(None, "tp")
    return jax.shard_map(
        on_device,
        mesh=mesh,
        in_specs=(rows, both, both, rows, rows) + (both,) * 6,
        out_specs=(both,) * 4 + (columns,) * 2 + (both,) * 4,
        check_vma=False,
    )
```

time: 77 us -> 63.2 us (0.82)
  local copies, waits for them, and re-layouts: 8.49 us -> 0 us
  Pallas kernels: 67.7 us -> 62.4 us
    pallas_call x1, Pallas kernels: 67.7 us -> 61 us  [on_device(): pl.pallas_call(functools.partial(kernel, float(2048 * 1024)), out_shape=(...]
    unnamed x24 -> x0, local copies, waits for them, and re-layouts: 4.76 us -> none
    slice x1 -> x0, local copies, waits for them, and re-layouts: 2.68 us -> none  [on_device(): copy_out = copies[1].reshape(2048, 256)]
    pallas_call x0 -> x1, Pallas kernels: none -> 1.42 us  [on_device(): pl.pallas_call(write_out, out_shape=(whole, whole) + (row,) * 4 + (pair,)...]
    transpose x1 -> x0, local copies, waits for them, and re-layouts: 1.04 us -> none  [on_device(): copy_in = jnp.swapaxes(copies[0], 0, 1).reshape(2048, 256)]
where the time goes in v2:
time: 63.2 us; the launch traced here: 63 us
  Pallas kernels  62.4 us (99%)
  between operations  0.65 us (1%)
    pallas_call x1, Pallas kernels, on_device(): pl.pallas_call(functools.partial(kernel, float(2048 * 1024)), out_shape=(...  61 us
    pallas_call x1, Pallas kernels, on_device(): pl.pallas_call(write_out, out_shape=(whole, whole) + (row,) * 4 + (pair,)...  1.42 us

profile of v2, /device:TPU:1, one launch (start us, length us, event | category | flops | bytes accessed | tf_op | source)
XLA Modules:
  0.0 63.0 jit_solution(15150361498751350842)
XLA Ops:
  0.6 61.0 %shard_map.186 = (bf16[2,8,8,32,256]{4,3,2,1,0:T(8,128)(2,1)S(1)}, f32[4,16,256]{2,1,0:T(8,128)S(1)}, f32[4,2,256]{2,1,0:T(2,128)S(1)}) custom-call(bf16[768,2048]{1,0:T(8,128)(2,1)} %saved.1, bf16[768,256]{1,0:T(8,128)(2,1)} %cot_in.1, bf16[768,256]{1,0:T(8,128)(2,1)} %cot_out.1, bf16[16,256]{1,0:T(8,128)(2,1)} %f_in.1, bf16[16,256]{1,0:T(8,128)(2,1)} %f_out.1, ...), custom_call_target="tpu_custom_call" | custom-call | tf_op jit(solution)/shard_map/pallas_call | solution.py:429
  61.6 1.4 %shard_map.187 = (bf16[8,8,32,256]{3,2,1,0:T(8,128)(2,1)}, bf16[8,8,32,256]{3,2,1,0:T(8,128)(2,1)}, f32[16,256]{1,0:T(8,128)}, f32[16,256]{1,0:T(8,128)}, f32[16...) custom-call(bf16[2,8,8,32,256]{4,3,2,1,0:T(8,128)(2,1)S(1)} %get-tup, ...), custom_call_target="tpu_custom_call" | custom-call | tf_op jit(solution)/shard_map/pallas_call | solution.py:441

commit v3 on v2

v3 whole, which is shorter than its diff:
```python
import functools
import math

import jax
import jax.numpy as jnp
from jax import lax
from jax.experimental import pallas as pl
from jax.experimental.pallas import tpu as pltpu
from jax.sharding import PartitionSpec as P

MESH = pl.DeviceIdType.MESH
F32 = jnp.float32
BF16 = jnp.bfloat16
FAR_FIRST = (4, 3, 5, 2, 6, 1, 7)
NEAR_FIRST = (1, 7, 2, 6, 3, 5, 4)
ROWS_FIRST = (((0,), (0,)), ((), ()))


def rank_order():
    r = lax.broadcasted_iota(jnp.int32, (256, 256), 0)
    p = lax.broadcasted_iota(jnp.int32, (256, 256), 1)
    target = ((r >> 2) & 7) * 32 + (r >> 5) * 4 + (r & 3)
    return jnp.where(target == p, 1.0, 0.0).astype(BF16)


def halves(value):
    high = value.astype(BF16)
    return high, (value - high.astype(F32)).astype(BF16)


def kernel(
    entries,
    saved, cot_in, cot_out, f_in, f_out, w_in, w_out, m1_in, m1_out, m2_in, m2_out,
    copies, rows, moments,
    s_v, c_v, fl, wl, r1, mo, mg, m1c, m2c,
    fg, go, gs, gr, spare, gh, gl, pp, rb, ab, sm, full, wg, qb, nst, nrx,
    load_sem, send_sem, a1_recv, mo_recv, w1_recv, w2_recv, near_recv, two_recv, three_recv, four_recv,
    fp_recv, wp_recv, g_recv, b2_recv, own_recv, b3_recv, c_recv, sp_recv, q_recv, n_recv,
):
    me, x = lax.axis_index("fs"), lax.axis_index("tp")
    c = lax.rem(me, 2)
    y = lax.rem(lax.div(me, 2), 8)
    z = lax.div(me, 16)
    u = z + c * (y - z)
    v = y + c * (z - y)
    other = 1 - c

    def plus(at, k):
        return lax.rem(at + k % 8, 8)

    def dev(zz, yy, cc):
        return ((zz * 8 + yy) * 2 + cc, x)

    def along_u(k, cc):
        to = plus(u, k)
        return dev(to + c * (v - to), v + c * (to - v), cc)

    def along_v(k):
        to = plus(v, k)
        return dev(u + c * (to - u), to + c * (u - to), c)

    partner = dev(z, y, other)
    sent = [0] * 7

    def send(src, dst, recv_sem, device, group):
        pltpu.make_async_remote_copy(
            src_ref=src, dst_ref=dst, send_sem=send_sem.at[group], recv_sem=recv_sem,
            device_id=device, device_id_type=MESH,
        ).start()
        sent[group] += math.prod(src.shape) * src.dtype.itemsize // 1024

    def arrive(dst, sem):
        pltpu.make_async_copy(dst, dst, sem).wait()

    barrier = pltpu.get_barrier_semaphore()
    peers = []
    for k in FAR_FIRST:
        for cc in range(2):
            peers.append(dev(plus(z, k), y, cc))
            peers.append(dev(z, plus(y, k), cc))
    for k in (2, 1, 3):
        peers.append((me, lax.rem(x + k, 4)))
        peers.append((me + 1 - 2 * c, lax.rem(x + k, 4)))
    peers.append(partner)
    for peer in peers:
        pl.semaphore_signal(barrier, inc=1, device_id=peer, device_id_type=MESH)

    def load(src, dst, group):
        copy = pltpu.make_async_copy(src, dst, load_sem.at[group])
        copy.start()
        return copy

    load(f_in, fl.at[0], 0)
    load(f_out, fl.at[1], 0)
    load(m1_in, r1.at[0], 1)
    load(m1_out, r1.at[1], 1)
    load(m2_in, r1.at[2], 1)
    load(m2_out, r1.at[3], 1)
    load(w_in, wl.at[0], 2)
    load(w_out, wl.at[1], 2)
    load(cot_in, c_v.at[:, pl.ds(pl.multiple_of(256 * c, 256), 256)], 3)
    load(cot_out, c_v.at[:, pl.ds(pl.multiple_of(256 * other, 256), 256)], 3)
    tokens = load(saved, s_v, 4)

    order = rank_order()
    arrive(fl, load_sem.at[0])
    fl[1] = jnp.dot(fl[1], order, preferred_element_type=F32).astype(BF16)
    fg[c, v, u, c] = fl[c]
    arrive(r1, load_sem.at[1])
    for X in range(2):
        mo[X, 0:2] = r1[X]
        mo[X, 2:4] = r1[2 + X]
    mg[0, y, 1] = mo[0]
    mg[1, z, 1] = mo[1]
    arrive(wl, load_sem.at[2])
    wg[c, v, u, c] = wl[c]
    pl.semaphore_wait(barrier, len(peers))

    def to_line(X, k):
        return dev(plus(z, k), y, 0) if X == 0 else dev(z, plus(y, k), 1)

    def to_cross(X, k):
        return dev(z, plus(y, k), 1) if X == 0 else dev(plus(z, k), y, 1)

    at_u, at_v = (z, y), (y, z)
    send(fl.at[other], fg.at[other, u, v, c], a1_recv.at[0], partner, 0)
    for k in FAR_FIRST:
        for X in range(2):
            send(fl.at[X], fg.at[X, at_v[X], at_u[X], c], a1_recv.at[k], to_line(X, k), 0)

    line = fg.at[c, v]

    def spread(k):
        block = line.at[plus(u, -k)]
        if k:
            arrive(block, a1_recv.at[k])
        else:
            arrive(fg.at[c, v, u, other], a1_recv.at[0])
        if k == 4:
            send(block, block, four_recv, along_v(4), 0)
            send(block, block, three_recv, along_v(3), 0)
            send(block, block, three_recv, along_v(-3), 0)
        send(block, block, two_recv.at[k], along_v(2), 0)
        send(block, block, two_recv.at[k], along_v(-2), 0)

    spread(0)
    send(wl.at[other], wg.at[other, u, v, c], w1_recv.at[0], partner, 0)
    for k in FAR_FIRST:
        for X in range(2):
            send(wl.at[X], wg.at[X, at_v[X], at_u[X], c], w1_recv.at[1], to_line(X, k), 0)

    arrive(c_v, load_sem.at[3])
    tokens.wait()

    def grad_copy(zc):
        return pltpu.make_async_remote_copy(
            src_ref=gs.at[zc], dst_ref=gr.at[zc], send_sem=send_sem.at[4], recv_sem=g_recv,
            device_id=partner, device_id_type=MESH,
        )

    def grad(zc, carry):
        at = pl.ds(pl.multiple_of(zc * 256, 256), 256)
        g = lax.dot_general(s_v[:, at], c_v[...], ROWS_FIRST, preferred_element_type=F32)
        gs[zc] = g[:, 256:512]
        go[zc] = g[:, 0:256]
        grad_copy(zc).start()
        return carry

    lax.fori_loop(0, 4, grad, 0)

    def relay(k, up):
        left, right = fg.at[c, plus(v, -2), plus(u, -k)], fg.at[c, plus(v, 2), plus(u, -k)]
        arrive(fg.at[c, v, pl.ds(0, 2)], two_recv.at[k])
        if up:
            send(left, left, four_recv, along_v(2), 0)
        else:
            send(right, right, four_recv, along_v(-2), 0)
        send(left, left, three_recv, along_v(1), 0)
        send(right, right, three_recv, along_v(-1), 0)

    def beside(k):
        block = line.at[plus(u, -k)]
        send(block, block, near_recv, along_v(1), 0)
        send(block, block, near_recv, along_v(-1), 0)

    beside(0)
    for k in (1, 7, 2, 6):
        spread(k)
        beside(k)
    relay(0, True)
    for k in (3, 5, 4):
        spread(k)

    lax.fori_loop(4, 6, grad, 0)

    for k in (1, 7, 2, 6):
        relay(k, k < 4)
    for k in (3, 5, 4):
        beside(k)
    lax.fori_loop(6, 8, grad, 0)
    for k in (3, 5):
        relay(k, k < 4)
    half = (pl.ds(0, 4), pl.ds(4, 4))

    def pass_weight(j):
        at = wg.at[c, plus(v, j)]
        send(at, at, wp_recv, partner, 3)

    def weight_step(s):
        a, b = plus(v, 1 - s), plus(v, s - 1)
        up, down = wg.at[c, a], wg.at[c, b]
        if s > 1:
            arrive(wg.at[c, pl.ds(0, 2)], w2_recv.at[s - 2])
        if s == 4:
            up, down = up.at[half[0]], down.at[half[1]]
        send(up, up, w2_recv.at[s - 1], along_v(1), 1)
        send(down, down, w2_recv.at[s - 1], along_v(-1), 1)
        pass_weight(1 - s)
        if s > 1:
            pass_weight(s - 1)

    arrive(wg.at[c, v, u, other], w1_recv.at[0])
    arrive(wg.at[c, v, pl.ds(0, 7)], w1_recv.at[1])
    weight_step(1)
    arrive(gr, g_recv)

    def combine(zc, carry):
        high, low = halves(go[zc] + gr[zc])
        for i in range(8):
            a, b = i + c * (zc - i), zc + c * (i - zc)
            gh[a, b] = high[32 * i:32 * i + 32]
            gl[a, b] = low[32 * i:32 * i + 32]
        return carry

    lax.fori_loop(0, 8, combine, 0)

    def project(j):
        f = fg[c, j].reshape(256, 256)
        term = lax.dot_general(f, gh[j].reshape(256, 256), ROWS_FIRST, preferred_element_type=F32)
        term += lax.dot_general(f, gl[j].reshape(256, 256), ROWS_FIRST, preferred_element_type=F32)
        return term.reshape(8, 32, 256)

    def pass_factor(j):
        at = fg.at[c, plus(v, j)]
        send(at, at, fp_recv, partner, 2)

    pass_factor(0)
    pp[...] = project(v)
    arrive(fg.at[c, pl.ds(0, 2)], near_recv)
    pp[...] += project(plus(v, -1))
    pp[...] += project(plus(v, 1))
    pass_factor(-1)
    pass_factor(1)
    arrive(fg.at[c, v, pl.ds(0, 2)], two_recv.at[4])
    pp[...] += project(plus(v, -2))
    pp[...] += project(plus(v, 2))
    pass_factor(-2)
    pass_factor(2)
    arrive(fg.at[c, pl.ds(0, 2)], three_recv)
    pp[...] += project(plus(v, -3))
    pp[...] += project(plus(v, 3))
    arrive(fg.at[c, 0], four_recv)
    pp[...] += project(plus(v, 4))
    for k in FAR_FIRST:
        send(pp.at[plus(u, k)], rb.at[c, u], b2_recv.at[c, k // 4 - k // 5], along_u(k, 1), 0)

    @pl.when(c == 0)
    def _():
        send(pp.at[u], rb.at[0, u], own_recv.at[0], partner, 5)
        for X in range(2):
            send(mo.at[X], mg.at[X, at_v[X], 0], mo_recv.at[0], partner, 5)

    pass_factor(-3)
    pass_factor(3)
    pass_factor(4)
    for k in FAR_FIRST:
        for X in range(2):
            send(mo.at[X], mg.at[X, at_v[X], c], mo_recv.at[1], to_cross(X, k), 0)

    weight_step(2)

    @pl.when(c == 1)
    def _():
        for X in (1, 0):
            arrive(rb.at[X, pl.ds(0, 6)], b2_recv.at[X, 0])
            arrive(rb.at[X, 0], b2_recv.at[X, 1])
            if X == 0:
                arrive(rb.at[0, 0], own_recv.at[0])
            total = rb[0, z] if X == 0 else pp[y]
            for k in NEAR_FIRST:
                total += rb[X, plus(at_u[X], -k)]
            mine = ab.at[X, at_v[X]]
            mine[...] = total
            for k in FAR_FIRST:
                send(mine, mine, b3_recv.at[X], to_cross(X, k), 6)
        arrive(mg.at[0, 0], mo_recv.at[0])
        arrive(mg.at[:, pl.ds(0, 7)], mo_recv.at[1])
        for X in range(2):
            for k in range(8):
                for cc in range(2):
                    at = 4 * k + 2 * cc
                    m1c[X, at:at + 2] = mg[X, k, cc, 0:2]
                    m2c[X, at:at + 2] = mg[X, k, cc, 2:4]

    weight_step(3)

    @pl.when(c == 1)
    def _():
        for X in (1, 0):
            arrive(ab.at[X, pl.ds(0, 7)], b3_recv.at[X])
            projected = ab[X, 0]
            for k in range(1, 8):
                projected += ab[X, k]
            first = 0.8 * m1c[X] + 0.2 * projected
            second = 0.9 * m2c[X] + 0.1 * projected * projected
            mine = sm.at[X, at_u[X]]
            mine[...] = first / (jnp.sqrt(second) + 1e-08)
            for k in FAR_FIRST:
                send(mine, mine, c_recv.at[min(k, 8 - k) - 1], to_line(X, k), 6)
            send(mine, mine, own_recv.at[1], partner, 6)
            m1c[X] = first
            m2c[X] = second
        for X in range(2):
            for i in range(2):
                at = 4 * at_v[X] + i
                nst[4 * X + i:4 * X + i + 1] = m1c[X, pl.ds(at, 1)]
                nst[4 * X + 2 + i:4 * X + 3 + i] = m2c[X, pl.ds(at, 1)]
                moments[X, i:i + 1] = m1c[X, pl.ds(at + 2, 1)]
                moments[2 + X, i:i + 1] = m2c[X, pl.ds(at + 2, 1)]
        send(nst, nrx, n_recv, partner, 6)

    weight_step(4)

    @pl.when(c == 0)
    def _():
        arrive(sm.at[0, pl.ds(0, 2)], own_recv.at[1])

    for k in (1, 2, 3, 4):
        pair = (k, -k) if k < 4 else (4,)
        arrive(sm.at[c, pl.ds(0, len(pair))], c_recv.at[k - 1])
        for i in pair:
            at = sm.at[c, plus(u, i)]
            send(at, at, sp_recv, partner, 2)

    def expanded(X):
        high, low = halves(sm[X].reshape(256, 256))
        small = jnp.concatenate([high, low], axis=0)

        def expand(j, squares):
            f = fg[X, j].reshape(256, 256)
            value = jnp.dot(jnp.concatenate([f, f], axis=1), small, preferred_element_type=F32)
            full[X, j] = value.reshape(8, 2, 16, 256)
            return squares + jnp.sum((value * value).reshape(32, 8, 256), axis=0)

        return lax.fori_loop(0, 8, expand, jnp.zeros((8, 256), F32), unroll=2)

    squares = expanded(c)
    qb[4 * c + x] = jnp.broadcast_to(jnp.sum(squares, keepdims=True), (8, 128))
    mine = qb.at[4 * c + x]
    for k in (2, 1, 3):
        to = lax.rem(x + k, 4)
        send(mine, mine, q_recv, (me, to), 2)
        send(mine, mine, q_recv, (me + 1 - 2 * c, to), 2)
    send(mine, mine, q_recv, partner, 2)
    four = wg.at[c, plus(v, 4)]
    arrive(four, w2_recv.at[3])
    pass_weight(4)
    arrive(fg.at[other], fp_recv)
    arrive(sm.at[other, pl.ds(0, 7)], sp_recv)
    expanded(other)
    arrive(qb.at[pl.ds(0, 7)], q_recv)

    def scale_of(X):
        square = ((qb[4 * X] + qb[4 * X + 1]) + qb[4 * X + 2]) + qb[4 * X + 3]
        scale = 1.0 / jnp.sqrt(square[0:1] / entries + 1e-06)
        return jnp.concatenate([scale, scale], axis=1)

    def finish(X, first_line, last_line):
        scale = scale_of(X)

        def line(j, carry):
            update = full[X, j].reshape(256, 256) * scale
            fresh = wg[X, j].reshape(256, 256) - 0.02 * update
            rounded = fresh.astype(BF16)
            for i in range(8):
                copies[X, i + X * (j - i), j + X * (i - j)] = rounded[32 * i:32 * i + 32]
            return carry

        lax.fori_loop(first_line, last_line, line, 0)

    finish(c, 0, 8)
    for X in range(2):
        update = full[X, at_v[X], at_u[X], c] * scale_of(X)
        rows[X] = update
        rows[2 + X] = wl[X] - 0.02 * update

    @pl.when(c == 0)
    def _():
        arrive(nrx, n_recv)
        for X in range(2):
            moments[X] = nrx[4 * X:4 * X + 2]
            moments[2 + X] = nrx[4 * X + 2:4 * X + 4]

    arrive(wg.at[other], wp_recv)
    finish(other, 0, 8)
    sent[4] = 2048

    def drained(group):
        arrive(spare.at[pl.ds(0, sent[group] // 4)], send_sem.at[group])

    for group in range(5):
        drained(group)
    pl.when(c == 0)(lambda: drained(5))
    pl.when(c == 1)(lambda: drained(6))


def write_out(copies, rows, moments, *refs):
    outs, sems = refs[:-1], refs[-1]
    sources = [copies.at[0], copies.at[1]] + [rows.at[i] for i in range(4)] + [moments.at[i] for i in range(4)]
    writes = [pltpu.make_async_copy(src, dst, sems.at[i]) for i, (src, dst) in enumerate(zip(sources, outs))]
    for write in writes:
        write.start()
    for write in writes:
        write.wait()


def on_device(*args):
    shape = jax.ShapeDtypeStruct
    dma = pltpu.SemaphoreType.DMA
    vmem = pltpu.VMEM
    anywhere = pl.BlockSpec(memory_space=pl.ANY)
    scratch = [
        vmem((768, 2048), BF16), vmem((768, 512), BF16),
        vmem((2, 16, 256), BF16), vmem((2, 16, 256), F32), vmem((4, 2, 256), F32),
        vmem((2, 8, 256), F32), vmem((2, 8, 2, 8, 256), F32),
        vmem((2, 32, 256), F32), vmem((2, 32, 256), F32),
        vmem((2, 8, 8, 2, 16, 256), BF16),
        vmem((8, 256, 256), F32), vmem((8, 256, 256), F32), vmem((8, 256, 256), F32), vmem((512, 8, 128), F32),
        vmem((8, 8, 32, 256), BF16), vmem((8, 8, 32, 256), BF16),
        vmem((8, 32, 256), F32), vmem((2, 8, 32, 256), F32),
        vmem((2, 8, 32, 256), F32), vmem((2, 8, 32, 256), F32),
        vmem((2, 8, 8, 2, 16, 256), F32), vmem((2, 8, 8, 2, 16, 256), F32),
        vmem((8, 8, 128), F32), vmem((8, 256), F32), vmem((8, 256), F32),
        dma((5,)), dma((7,)), dma((8,)), dma((2,)), dma((2,)), dma((4,)), dma(()), dma((8,)), dma(()), dma(()),
        dma(()), dma(()), dma(()), dma((2, 2)), dma((2,)), dma((2,)), dma((4,)), dma(()), dma(()), dma(()),
    ]
    mid = pl.pallas_call(
        functools.partial(kernel, float(2048 * 1024)),
        out_shape=(shape((2, 8, 8, 32, 256), BF16), shape((4, 16, 256), F32), shape((4, 2, 256), F32)),
        in_specs=[pl.BlockSpec(memory_space=pltpu.HBM)] * 11,
        out_specs=(pl.BlockSpec(memory_space=pltpu.VMEM),) * 3,
        scratch_shapes=scratch,
        compiler_params=pltpu.CompilerParams(
            collective_id=0, has_side_effects=True, vmem_limit_bytes=40 * 1024 * 1024
        ),
    )(*(pltpu.with_memory_space_constraint(a, pltpu.HBM) for a in args))
    mid = [pltpu.with_memory_space_constraint(m, pltpu.VMEM) for m in mid]
    whole, row, pair = shape((8, 8, 32, 256), BF16), shape((16, 256), F32), shape((2, 256), F32)
    copy_in, copy_out, *rest = pl.pallas_call(
        write_out,
        out_shape=(whole, whole) + (row,) * 4 + (pair,) * 4,
        in_specs=[pl.BlockSpec(memory_space=pltpu.VMEM)] * 3,
        out_specs=(anywhere,) * 10,
        scratch_shapes=[dma((10,))],
    )(*mid)
    return (*rest[:4], copy_in.reshape(2048, 256), copy_out.reshape(2048, 256), *rest[4:])


def solution(mesh):
    both, rows, columns = P("fs", "tp"), P("fs", None), P(None, "tp")
    return jax.shard_map(
        on_device,
        mesh=mesh,
        in_specs=(rows, both, both, rows, rows) + (both,) * 6,
        out_specs=(both,) * 4 + (columns,) * 2 + (both,) * 4,
        check_vma=False,
    )
```

time: 63.2 us -> 60 us (0.949)
  Pallas kernels: 62.4 us -> 59.2 us
    pallas_call x1, Pallas kernels: 61 us -> 57.8 us  [on_device(): pl.pallas_call(functools.partial(kernel, float(2048 * 1024)), out_shape=(...]
where the time goes in v3:
time: 60 us; the launch traced here: 59.9 us
  Pallas kernels  59.2 us (99%)
  between operations  0.65 us (1%)
    pallas_call x1, Pallas kernels, on_device(): pl.pallas_call(functools.partial(kernel, float(2048 * 1024)), out_shape=(...  57.8 us
    pallas_call x1, Pallas kernels, on_device(): pl.pallas_call(write_out, out_shape=(whole, whole) + (row,) * 4 + (pair,)...  1.42 us

profile of v3, /device:TPU:1, one launch (start us, length us, event | category | flops | bytes accessed | tf_op | source)
XLA Modules:
  0.0 59.9 jit_solution(9580043036541221240)
XLA Ops:
  0.6 57.8 %shard_map.186 = (bf16[2,8,8,32,256]{4,3,2,1,0:T(8,128)(2,1)S(1)}, f32[4,16,256]{2,1,0:T(8,128)S(1)}, f32[4,2,256]{2,1,0:T(2,128)S(1)}) custom-call(bf16[768,2048]{1,0:T(8,128)(2,1)} %saved.1, bf16[768,256]{1,0:T(8,128)(2,1)} %cot_in.1, bf16[768,256]{1,0:T(8,128)(2,1)} %cot_out.1, bf16[16,256]{1,0:T(8,128)(2,1)} %f_in.1, bf16[16,256]{1,0:T(8,128)(2,1)} %f_out.1, ...), custom_call_target="tpu_custom_call" | custom-call | tf_op jit(solution)/shard_map/pallas_call | solution.py:447
  58.5 1.4 %shard_map.187 = (bf16[8,8,32,256]{3,2,1,0:T(8,128)(2,1)}, bf16[8,8,32,256]{3,2,1,0:T(8,128)(2,1)}, f32[16,256]{1,0:T(8,128)}, f32[16,256]{1,0:T(8,128)}, f32[16...) custom-call(bf16[2,8,8,32,256]{4,3,2,1,0:T(8,128)(2,1)S(1)} %get-tup, ...), custom_call_target="tpu_custom_call" | custom-call | tf_op jit(solution)/shard_map/pallas_call | solution.py:459

commit v4 on v3

--- a/solution.py
+++ b/solution.py
@@ -28,12 +28,18 @@
     return high, (value - high.astype(F32)).astype(BF16)
 
 
+def thirds(value):
+    high = value.astype(BF16)
+    rest = value - high.astype(F32)
+    middle = rest.astype(BF16)
+    return high, middle, (rest - middle.astype(F32)).astype(BF16)
+
+
 def kernel(
-    entries,
     saved, cot_in, cot_out, f_in, f_out, w_in, w_out, m1_in, m1_out, m2_in, m2_out,
-    copies, rows, moments,
+    full, wg, qb, moments,
     s_v, c_v, fl, wl, r1, mo, mg, m1c, m2c,
-    fg, go, gs, gr, spare, gh, gl, pp, rb, ab, sm, full, wg, qb, nst, nrx,
+    fg, go, gs, gr, spare, gh, gl, pp, rb, ab, sm, nst, nrx, gm,
     load_sem, send_sem, a1_recv, mo_recv, w1_recv, w2_recv, near_recv, two_recv, three_recv, four_recv,
     fp_recv, wp_recv, g_recv, b2_recv, own_recv, b3_recv, c_recv, sp_recv, q_recv, n_recv,
 ):
@@ -190,17 +196,25 @@
     relay(0, True)
     for k in (3, 5, 4):
         spread(k)
-
-    lax.fori_loop(4, 6, grad, 0)
+    for k in (3, 5, 4):
+        beside(k)
+
+    lax.fori_loop(4, 8, grad, 0)
 
     for k in (1, 7, 2, 6):
         relay(k, k < 4)
-    for k in (3, 5, 4):
-        beside(k)
-    lax.fori_loop(6, 8, grad, 0)
     for k in (3, 5):
         relay(k, k < 4)
-    half = (pl.ds(0, 4), pl.ds(4, 4))
+    for k in FAR_FIRST:
+        for X in range(2):
+            send(mo.at[X], mg.at[X, at_v[X], c], mo_recv.at[1], to_cross(X, k), 0)
+
+    @pl.when(c == 0)
+    def _():
+        for X in range(2):
+            send(mo.at[X], mg.at[X, at_v[X], 0], mo_recv.at[0], partner, 5)
+
+    parts = [pl.ds(2 * i, 2) for i in range(4)]
 
     def pass_weight(j):
         at = wg.at[c, plus(v, j)]
@@ -209,12 +223,13 @@
     def weight_step(s):
         a, b = plus(v, 1 - s), plus(v, s - 1)
         up, down = wg.at[c, a], wg.at[c, b]
-        if s > 1:
-            arrive(wg.at[c, pl.ds(0, 2)], w2_recv.at[s - 2])
-        if s == 4:
-            up, down = up.at[half[0]], down.at[half[1]]
-        send(up, up, w2_recv.at[s - 1], along_v(1), 1)
-        send(down, down, w2_recv.at[s - 1], along_v(-1), 1)
+        for i, part in enumerate(parts):
+            if s > 1:
+                arrive(wg.at[c, v, pl.ds(0, 4)], w2_recv.at[s - 2, i])
+            if s < 4 or i < 2:
+                send(up.at[part], up.at[part], w2_recv.at[s - 1, i], along_v(1), 1)
+            if s < 4 or i > 1:
+                send(down.at[part], down.at[part], w2_recv.at[s - 1, i], along_v(-1), 1)
         pass_weight(1 - s)
         if s > 1:
             pass_weight(s - 1)
@@ -267,16 +282,18 @@
     @pl.when(c == 0)
     def _():
         send(pp.at[u], rb.at[0, u], own_recv.at[0], partner, 5)
-        for X in range(2):
-            send(mo.at[X], mg.at[X, at_v[X], 0], mo_recv.at[0], partner, 5)
 
     pass_factor(-3)
     pass_factor(3)
     pass_factor(4)
-    for k in FAR_FIRST:
-        for X in range(2):
-            send(mo.at[X], mg.at[X, at_v[X], c], mo_recv.at[1], to_cross(X, k), 0)
-
+    def squared(j, total):
+        f = fg[c, j].reshape(256, 256)
+        return total + lax.dot_general(f, f, ROWS_FIRST, preferred_element_type=F32)
+
+    gram = lax.fori_loop(0, 8, squared, jnp.zeros((256, 256), F32))
+    for i, part in enumerate(thirds(gram)):
+        for at in ((0, 256, 1024), (512, 768), (1280,))[i]:
+            gm[:, at:at + 256] = part
     weight_step(2)
 
     @pl.when(c == 1)
@@ -342,19 +359,10 @@
             at = sm.at[c, plus(u, i)]
             send(at, at, sp_recv, partner, 2)
 
-    def expanded(X):
-        high, low = halves(sm[X].reshape(256, 256))
-        small = jnp.concatenate([high, low], axis=0)
-
-        def expand(j, squares):
-            f = fg[X, j].reshape(256, 256)
-            value = jnp.dot(jnp.concatenate([f, f], axis=1), small, preferred_element_type=F32)
-            full[X, j] = value.reshape(8, 2, 16, 256)
-            return squares + jnp.sum((value * value).reshape(32, 8, 256), axis=0)
-
-        return lax.fori_loop(0, 8, expand, jnp.zeros((8, 256), F32), unroll=2)
-
-    squares = expanded(c)
+    small = sm[c].reshape(256, 256)
+    high, middle, low = thirds(small)
+    spread_small = jnp.concatenate([high, middle, high, middle, low, high], axis=0)
+    squares = small * jnp.dot(gm[...], spread_small, preferred_element_type=F32)
     qb[4 * c + x] = jnp.broadcast_to(jnp.sum(squares, keepdims=True), (8, 128))
     mine = qb.at[4 * c + x]
     for k in (2, 1, 3):
@@ -362,38 +370,29 @@
         send(mine, mine, q_recv, (me, to), 2)
         send(mine, mine, q_recv, (me + 1 - 2 * c, to), 2)
     send(mine, mine, q_recv, partner, 2)
+
+    def expanded(X):
+        high, low = halves(sm[X].reshape(256, 256))
+        small = jnp.concatenate([high, low], axis=0)
+
+        def expand(j, carry):
+            f = fg[X, j].reshape(256, 256)
+            value = jnp.dot(jnp.concatenate([f, f], axis=1), small, preferred_element_type=F32)
+            full[X, j] = value.reshape(8, 2, 16, 256)
+            return carry
+
+        lax.fori_loop(0, 8, expand, 0, unroll=2)
+
+    expanded(c)
     four = wg.at[c, plus(v, 4)]
-    arrive(four, w2_recv.at[3])
+    for i, part in enumerate(parts):
+        arrive(four.at[part], w2_recv.at[3, i])
     pass_weight(4)
     arrive(fg.at[other], fp_recv)
     arrive(sm.at[other, pl.ds(0, 7)], sp_recv)
     expanded(other)
     arrive(qb.at[pl.ds(0, 7)], q_recv)
 
-    def scale_of(X):
-        square = ((qb[4 * X] + qb[4 * X + 1]) + qb[4 * X + 2]) + qb[4 * X + 3]
-        scale = 1.0 / jnp.sqrt(square[0:1] / entries + 1e-06)
-        return jnp.concatenate([scale, scale], axis=1)
-
-    def finish(X, first_line, last_line):
-        scale = scale_of(X)
-
-        def line(j, carry):
-            update = full[X, j].reshape(256, 256) * scale
-            fresh = wg[X, j].reshape(256, 256) - 0.02 * update
-            rounded = fresh.astype(BF16)
-            for i in range(8):
-                copies[X, i + X * (j - i), j + X * (i - j)] = rounded[32 * i:32 * i + 32]
-            return carry
-
-        lax.fori_loop(first_line, last_line, line, 0)
-
-    finish(c, 0, 8)
-    for X in range(2):
-        update = full[X, at_v[X], at_u[X], c] * scale_of(X)
-        rows[X] = update
-        rows[2 + X] = wl[X] - 0.02 * update
-
     @pl.when(c == 0)
     def _():
         arrive(nrx, n_recv)
@@ -402,7 +401,6 @@
             moments[2 + X] = nrx[4 * X + 2:4 * X + 4]
 
     arrive(wg.at[other], wp_recv)
-    finish(other, 0, 8)
     sent[4] = 2048
 
     def drained(group):
@@ -414,14 +412,47 @@
     pl.when(c == 1)(lambda: drained(6))
 
 
-def write_out(copies, rows, moments, *refs):
-    outs, sems = refs[:-1], refs[-1]
-    sources = [copies.at[0], copies.at[1]] + [rows.at[i] for i in range(4)] + [moments.at[i] for i in range(4)]
-    writes = [pltpu.make_async_copy(src, dst, sems.at[i]) for i, (src, dst) in enumerate(zip(sources, outs))]
-    for write in writes:
-        write.start()
-    for write in writes:
-        write.wait()
+def write_out(
+    entries, full, wg, qb, moments,
+    copy_in, copy_out, upd_in, upd_out, new_in, new_out, fst_in, fst_out, snd_in, snd_out,
+    copies, rows, sems,
+):
+    me = lax.axis_index("fs")
+    c = lax.rem(me, 2)
+    y = lax.rem(lax.div(me, 2), 8)
+    z = lax.div(me, 16)
+    writes = []
+
+    def write(src, dst):
+        writes.append(pltpu.make_async_copy(src, dst, sems.at[len(writes)]))
+        writes[-1].start()
+
+    for i, dst in enumerate((fst_in, fst_out, snd_in, snd_out)):
+        write(moments.at[i], dst)
+    for X in range(2):
+        square = ((qb[4 * X] + qb[4 * X + 1]) + qb[4 * X + 2]) + qb[4 * X + 3]
+        scale = 1.0 / jnp.sqrt(square[0:1] / entries + 1e-06)
+        scale = jnp.concatenate([scale, scale], axis=1)
+
+        def line(j, carry):
+            update = full[X, j].reshape(256, 256) * scale
+            fresh = wg[X, j].reshape(256, 256) - 0.02 * update
+            copies[X, j] = fresh.astype(BF16).reshape(8, 32, 256)
+            dst = copy_out.at[j] if X else copy_in.at[:, j]
+            pltpu.make_async_copy(copies.at[X, j], dst, sems.at[8 + X]).start()
+            return carry
+
+        lax.fori_loop(0, 8, line, 0)
+        at = (z, y, c) if X else (y, z, c)
+        update = full[X, at[0], at[1], at[2]] * scale
+        rows[X] = update
+        rows[2 + X] = wg[X, at[0], at[1], at[2]] - 0.02 * update
+        write(rows.at[X], upd_out if X else upd_in)
+        write(rows.at[2 + X], new_out if X else new_in)
+    for copy in writes:
+        copy.wait()
+    for X in range(2):
+        pltpu.make_async_copy(copies.at[X], copies.at[X], sems.at[8 + X]).wait()
 
 
 def on_device(*args):
@@ -432,23 +463,23 @@
     scratch = [
         vmem((768, 2048), BF16), vmem((768, 512), BF16),
         vmem((2, 16, 256), BF16), vmem((2, 16, 256), F32), vmem((4, 2, 256), F32),
-        vmem((2, 8, 256), F32), vmem((2, 8, 2, 8, 256), F32),
+        vmem((2, 4, 256), F32), vmem((2, 8, 2, 4, 256), F32),
         vmem((2, 32, 256), F32), vmem((2, 32, 256), F32),
         vmem((2, 8, 8, 2, 16, 256), BF16),
         vmem((8, 256, 256), F32), vmem((8, 256, 256), F32), vmem((8, 256, 256), F32), vmem((512, 8, 128), F32),
         vmem((8, 8, 32, 256), BF16), vmem((8, 8, 32, 256), BF16),
         vmem((8, 32, 256), F32), vmem((2, 8, 32, 256), F32),
         vmem((2, 8, 32, 256), F32), vmem((2, 8, 32, 256), F32),
-        vmem((2, 8, 8, 2, 16, 256), F32), vmem((2, 8, 8, 2, 16, 256), F32),
-        vmem((8, 8, 128), F32), vmem((8, 256), F32), vmem((8, 256), F32),
-        dma((5,)), dma((7,)), dma((8,)), dma((2,)), dma((2,)), dma((4,)), dma(()), dma((8,)), dma(()), dma(()),
+        vmem((8, 256), F32), vmem((8, 256), F32), vmem((256, 1536), BF16),
+        dma((5,)), dma((7,)), dma((8,)), dma((2,)), dma((2,)), dma((4, 4)), dma(()), dma((8,)), dma(()), dma(()),
         dma(()), dma(()), dma(()), dma((2, 2)), dma((2,)), dma((2,)), dma((4,)), dma(()), dma(()), dma(()),
     ]
+    lines = shape((2, 8, 8, 2, 16, 256), F32)
     mid = pl.pallas_call(
-        functools.partial(kernel, float(2048 * 1024)),
-        out_shape=(shape((2, 8, 8, 32, 256), BF16), shape((4, 16, 256), F32), shape((4, 2, 256), F32)),
+        kernel,
+        out_shape=(lines, lines, shape((8, 8, 128), F32), shape((4, 2, 256), F32)),
         in_specs=[pl.BlockSpec(memory_space=pltpu.HBM)] * 11,
-        out_specs=(pl.BlockSpec(memory_space=pltpu.VMEM),) * 3,
+        out_specs=(pl.BlockSpec(memory_space=pltpu.VMEM),) * 4,
         scratch_shapes=scratch,
         compiler_params=pltpu.CompilerParams(
             collective_id=0, has_side_effects=True, vmem_limit_bytes=40 * 1024 * 1024
@@ -457,11 +488,12 @@
     mid = [pltpu.with_memory_space_constraint(m, pltpu.VMEM) for m in mid]
     whole, row, pair = shape((8, 8, 32, 256), BF16), shape((16, 256), F32), shape((2, 256), F32)
     copy_in, copy_out, *rest = pl.pallas_call(
-        write_out,
+        functools.partial(write_out, float(2048 * 1024)),
         out_shape=(whole, whole) + (row,) * 4 + (pair,) * 4,
-        in_specs=[pl.BlockSpec(memory_space=pltpu.VMEM)] * 3,
+        in_specs=[pl.BlockSpec(memory_space=pltpu.VMEM)] * 4,
         out_specs=(anywhere,) * 10,
-        scratch_shapes=[dma((10,))],
+        scratch_shapes=[vmem((2, 8, 8, 32, 256), BF16), vmem((4, 16, 256), F32), dma((10,))],
+        compiler_params=pltpu.CompilerParams(vmem_limit_bytes=16 * 1024 * 1024),
     )(*mid)
     return (*rest[:4], copy_in.reshape(2048, 256), copy_out.reshape(2048, 256), *rest[4:])
 

time: 60 us -> 57 us (0.950)
  Pallas kernels: 59.2 us -> 56.2 us
    pallas_call x2, Pallas kernels: 59.2 us -> 56.2 us  [the longest x1 54.8 us: on_device(): pl.pallas_call(kernel, out_shape=(lines, lines, shape((8, 8, 128), F32),...]
where the time goes in v4:
time: 57 us; the launch traced here: 56.9 us
  Pallas kernels  56.2 us (99%)
  between operations  0.65 us (1%)
    pallas_call x1, Pallas kernels, on_device(): pl.pallas_call(kernel, out_shape=(lines, lines, shape((8, 8, 128), F32),...  54.8 us
    pallas_call x1, Pallas kernels, on_device(): pl.pallas_call(functools.partial(write_out, float(2048 * 1024)), out_shap...  1.45 us

profile of v4, /device:TPU:1, one launch (start us, length us, event | category | flops | bytes accessed | tf_op | source)
XLA Modules:
  0.0 56.9 jit_solution(7704907171048592184)
XLA Ops:
  0.6 54.8 %shard_map.186 = (f32[2,8,8,2,16,256]{5,4,3,2,1,0:T(8,128)S(1)}, f32[2,8,8,2,16,256]{5,4,3,2,1,0:T(8,128)S(1)}, f32[8,8,128]{2,1,0:T(8,128)S(1)}, f32[4,2,256]{2,1,0:T(2,128)S(1)}) custom-call(bf16[768,2048]{1,0:T(8,128)(2,1)} %saved.1, bf16[768,256]{1,0:T(8,128)(2,1)} %cot_in.1, bf16[768,256]{1,0:T(8,128)(2,1)} %cot_out.1, bf16[16,256]{1,0:T(8,128)(2,1)} %f_in.1, ...), custom_call_target="tpu_custom_call" | custom-call | tf_op jit(solution)/shard_map/pallas_call | solution.py:478
  55.4 1.5 %shard_map.187 = (bf16[8,8,32,256]{3,2,1,0:T(8,128)(2,1)}, bf16[8,8,32,256]{3,2,1,0:T(8,128)(2,1)}, f32[16,256]{1,0:T(8,128)}, f32[16,256]{1,0:T(8,128)}, f32[16...) custom-call(f32[2,8,8,2,16,256]{5,4,3,2,1,0:T(8,128)S(1)} %get-tuple, ...), custom_call_target="tpu_custom_call" | custom-call | tf_op jit(solution)/shard_map/pallas_call | solution.py:490

commit v5 on v4

--- a/solution.py
+++ b/solution.py
@@ -214,7 +214,7 @@
         for X in range(2):
             send(mo.at[X], mg.at[X, at_v[X], 0], mo_recv.at[0], partner, 5)
 
-    parts = [pl.ds(2 * i, 2) for i in range(4)]
+    parts = [pl.ds(4 * i, 4) for i in range(2)]
 
     def pass_weight(j):
         at = wg.at[c, plus(v, j)]
@@ -225,10 +225,10 @@
         up, down = wg.at[c, a], wg.at[c, b]
         for i, part in enumerate(parts):
             if s > 1:
-                arrive(wg.at[c, v, pl.ds(0, 4)], w2_recv.at[s - 2, i])
-            if s < 4 or i < 2:
+                arrive(wg.at[c, v], w2_recv.at[s - 2, i])
+            if s < 4 or i == 0:
                 send(up.at[part], up.at[part], w2_recv.at[s - 1, i], along_v(1), 1)
-            if s < 4 or i > 1:
+            if s < 4 or i == 1:
                 send(down.at[part], down.at[part], w2_recv.at[s - 1, i], along_v(-1), 1)
         pass_weight(1 - s)
         if s > 1:
@@ -429,22 +429,25 @@
 
     for i, dst in enumerate((fst_in, fst_out, snd_in, snd_out)):
         write(moments.at[i], dst)
+    scales = []
     for X in range(2):
         square = ((qb[4 * X] + qb[4 * X + 1]) + qb[4 * X + 2]) + qb[4 * X + 3]
         scale = 1.0 / jnp.sqrt(square[0:1] / entries + 1e-06)
-        scale = jnp.concatenate([scale, scale], axis=1)
-
-        def line(j, carry):
-            update = full[X, j].reshape(256, 256) * scale
+        scales.append(jnp.concatenate([scale, scale], axis=1))
+
+    def line(j, carry):
+        for X in range(2):
+            update = full[X, j].reshape(256, 256) * scales[X]
             fresh = wg[X, j].reshape(256, 256) - 0.02 * update
             copies[X, j] = fresh.astype(BF16).reshape(8, 32, 256)
             dst = copy_out.at[j] if X else copy_in.at[:, j]
             pltpu.make_async_copy(copies.at[X, j], dst, sems.at[8 + X]).start()
-            return carry
-
-        lax.fori_loop(0, 8, line, 0)
+        return carry
+
+    lax.fori_loop(0, 8, line, 0, unroll=2)
+    for X in range(2):
         at = (z, y, c) if X else (y, z, c)
-        update = full[X, at[0], at[1], at[2]] * scale
+        update = full[X, at[0], at[1], at[2]] * scales[X]
         rows[X] = update
         rows[2 + X] = wg[X, at[0], at[1], at[2]] - 0.02 * update
         write(rows.at[X], upd_out if X else upd_in)
@@ -471,7 +474,7 @@
         vmem((8, 32, 256), F32), vmem((2, 8, 32, 256), F32),
         vmem((2, 8, 32, 256), F32), vmem((2, 8, 32, 256), F32),
         vmem((8, 256), F32), vmem((8, 256), F32), vmem((256, 1536), BF16),
-        dma((5,)), dma((7,)), dma((8,)), dma((2,)), dma((2,)), dma((4, 4)), dma(()), dma((8,)), dma(()), dma(()),
+        dma((5,)), dma((7,)), dma((8,)), dma((2,)), dma((2,)), dma((4, 2)), dma(()), dma((8,)), dma(()), dma(()),
         dma(()), dma(()), dma(()), dma((2, 2)), dma((2,)), dma((2,)), dma((4,)), dma(()), dma(()), dma(()),
     ]
     lines = shape((2, 8, 8, 2, 16, 256), F32)

time: 57 us -> 56.9 us (level)
  no operation moved by 1% of the time
where the time goes in v5:
time: 56.9 us; the launch traced here: 56.8 us
  Pallas kernels  56.1 us (99%)
  between operations  0.65 us (1%)
    pallas_call x1, Pallas kernels, on_device(): pl.pallas_call(kernel, out_shape=(lines, lines, shape((8, 8, 128), F32),...  54.7 us
    pallas_call x1, Pallas kernels, on_device(): pl.pallas_call(functools.partial(write_out, float(2048 * 1024)), out_shap...  1.45 us

profile of v5, /device:TPU:1, one launch (start us, length us, event | category | flops | bytes accessed | tf_op | source)
XLA Modules:
  0.0 56.8 jit_solution(10150647244621849599)
XLA Ops:
  0.6 54.7 %shard_map.186 = (f32[2,8,8,2,16,256]{5,4,3,2,1,0:T(8,128)S(1)}, f32[2,8,8,2,16,256]{5,4,3,2,1,0:T(8,128)S(1)}, f32[8,8,128]{2,1,0:T(8,128)S(1)}, f32[4,2,256]{2,1,0:T(2,128)S(1)}) custom-call(bf16[768,2048]{1,0:T(8,128)(2,1)} %saved.1, bf16[768,256]{1,0:T(8,128)(2,1)} %cot_in.1, bf16[768,256]{1,0:T(8,128)(2,1)} %cot_out.1, bf16[16,256]{1,0:T(8,128)(2,1)} %f_in.1, ...), custom_call_target="tpu_custom_call" | custom-call | tf_op jit(solution)/shard_map/pallas_call | solution.py:481
  55.3 1.5 %shard_map.187 = (bf16[8,8,32,256]{3,2,1,0:T(8,128)(2,1)}, bf16[8,8,32,256]{3,2,1,0:T(8,128)(2,1)}, f32[16,256]{1,0:T(8,128)}, f32[16,256]{1,0:T(8,128)}, f32[16...) custom-call(f32[2,8,8,2,16,256]{5,4,3,2,1,0:T(8,128)S(1)} %get-tuple, ...), custom_call_target="tpu_custom_call" | custom-call | tf_op jit(solution)/shard_map/pallas_call | solution.py:493
